TPU v7x, 32 devices: a whole 2x2x4 slice. The times are simulated.
32 devices in a mesh: sp: 8 (over z, y), tp: 4 (over x, core).
Axes of the slice: x: 2, y: 2, z: 4, core: 2. Of those that a mesh axis runs over, the one named last changes fastest.
Arguments:
- stream: bfloat16 [2048, 2048], P('sp'), may hold values from -6 to 6
- pooled_in: bfloat16 [2048, 1024], P('sp', 'tp'), may hold values from -6 to 6
- pool_weight: bfloat16 [4, 256, 256], P('tp'), may hold values from -0.375 to 0.375
- pool_scale: float32 [1024], P('tp'), may hold values from 0.1 to 1.9
- out_weight: bfloat16 [1024, 2048], replicated, may hold values from -0.1875 to 0.1875
- norm_gain: float32 [2048], replicated, may hold values from 0.1 to 1.9
- routes: int32 [2048, 3], P('sp'), may hold values from 0 to 7, all different within a row; in each aligned block of 64 rows (0 to 63, 64 to 127, ...) at most 48 rows name the same one
- route_weights: float32 [2048, 3], P('sp'), may hold values from 0.25 to 2.5
- expert_gate: bfloat16 [8, 2048, 2048], P('sp', None, 'tp'), may hold values from -0.125 to 0.125
- expert_up: bfloat16 [8, 2048, 2048], P('sp', None, 'tp'), may hold values from -0.125 to 0.125
- expert_down: bfloat16 [8, 2048, 2048], P('sp', 'tp'), may hold values from -0.125 to 0.125
- shared_gate: bfloat16 [2048, 512], P(None, 'tp'), may hold values from -0.125 to 0.125
- shared_up: bfloat16 [2048, 512], P(None, 'tp'), may hold values from -0.125 to 0.125
- shared_down: bfloat16 [512, 2048], P('tp'), may hold values from -0.25 to 0.25
Outputs:
- layer_out: bfloat16 [2048, 2048], P(('sp', 'tp'))
Inputs may be any that keep to these rules, and one draw needn't show every extreme that they name: `routes`: each row names 3 different experts. In each aligned block of 64 rows (the rows of one device in the layer's output) no expert is named by more than 48 rows, a bound that some block reaches.
All inputs are finite; a program needn't handle non-finite values.
Results may differ from a plain program's by a relative error of at most 0.012.
Values may be sent and summed in bfloat16 or wider, within the bound.
No kernel may reach another device: no remote copies, remote signals or barrier semaphores. Data moves between devices by JAX's collectives and lax.ppermute only.
A program may use at most 128 MiB of HBM per device.

v0:
```python
import functools

import jax
import jax.numpy as jnp
from jax import lax
from jax.experimental import pallas as pl
from jax.experimental.pallas import tpu as pltpu
from jax.sharding import PartitionSpec as P


REACH = 16


EPSILON = 1e-06

AXES = ("sp", "tp")
CORE_BIT, X_BIT = 1, 2
MIB = 2**20


def passed_along(value, axis, steps):
    count = lax.axis_size(axis)
    initial, last = (max(0, -steps), min(count, count - steps))
    return lax.ppermute(value, axis, [(source, source + steps) for source in range(initial, last)])


def swapped(value, flip):
    count = lax.axis_size(AXES)
    return lax.ppermute(value, AXES, [(source, source ^ flip) for source in range(count)])


def slot_positions(route_block, n_experts, capacity):
    flat_ids = route_block.reshape(-1)
    onehot = (flat_ids[:, None] == jnp.arange(n_experts, dtype=jnp.int32)[None, :]).astype(
        jnp.int32
    )
    earlier = jnp.cumsum(onehot, axis=0) - onehot
    rank_in = jnp.sum(earlier * onehot, axis=1)
    return flat_ids * capacity + rank_in


def mixer(stream, pooled_in, pool_weight, pool_scale, out_weight, norm_gain):
    tok_dev, group_width = pooled_in.shape
    tp_index = lax.axis_index("tp")
    sp_index = lax.axis_index("sp")
    window = lax.shift_left(jnp.int32(2), tp_index)
    rim_rows = passed_along(pooled_in[tok_dev - (REACH - 1) :], "sp", 1)
    padded = jnp.concatenate([rim_rows, pooled_in], 0).astype(jnp.float32)
    summed = jnp.zeros((tok_dev, group_width), jnp.float32)
    for lag_step in range(REACH):
        enabled = (lag_step < window).astype(jnp.float32)
        summed = summed + padded[REACH - 1 - lag_step : REACH - 1 - lag_step + tok_dev] * enabled
    position = sp_index * tok_dev + jnp.arange(tok_dev, dtype=jnp.int32)
    counted = jnp.minimum(position + 1, window).astype(jnp.float32)
    pooled = (summed / counted[:, None] - padded[REACH - 1 :]).astype(jnp.bfloat16)
    group_mix = (
        jnp.dot(pooled, pool_weight[0], preferred_element_type=jnp.float32) * pool_scale
    ).astype(jnp.bfloat16)
    mixed_all = jnp.dot(
        lax.all_gather(group_mix, "tp", axis=1, tiled=True),
        out_weight,
        preferred_element_type=jnp.float32,
    )
    residual = (stream.astype(jnp.float32) + mixed_all).astype(jnp.bfloat16)
    resid_wide = residual.astype(jnp.float32)
    normed = (
        resid_wide
        * lax.rsqrt(jnp.mean(resid_wide * resid_wide, axis=-1, keepdims=True) + EPSILON)
        * norm_gain
    ).astype(jnp.bfloat16)
    return residual, normed


def gated(rows_in, gate, up):
    return (
        jax.nn.silu(jnp.dot(rows_in, gate, preferred_element_type=jnp.float32))
        * jnp.dot(rows_in, up, preferred_element_type=jnp.float32)
    ).astype(jnp.bfloat16)


def routed_plan(
    residual, normed, routes, route_weights, expert_gate, expert_up, expert_down,
    shared_gate, shared_up, shared_down,
):
    tok_dev, model_width = residual.shape
    tp_size = lax.axis_size("tp")
    sp_size = lax.axis_size("sp")
    tp_index = lax.axis_index("tp")
    top_count = routes.shape[1]
    rows_dev = tok_dev // tp_size
    capacity = max(2, 2 * rows_dev * top_count // sp_size)
    own_begin = tp_index * rows_dev
    own_routes = lax.dynamic_slice_in_dim(routes, own_begin, rows_dev, 0)
    own_pos = slot_positions(own_routes, sp_size, capacity)
    own_normed = lax.dynamic_slice_in_dim(normed, own_begin, rows_dev, 0)
    sending = jnp.zeros((sp_size * capacity, model_width), jnp.bfloat16)
    sending = sending.at[own_pos].set(jnp.repeat(own_normed, top_count, axis=0))
    landed = lax.all_to_all(
        sending.reshape(sp_size, capacity, model_width),
        "sp",
        split_axis=0,
        concat_axis=0,
        tiled=True,
    )
    arrived = lax.all_gather(landed[None], "tp", axis=0, tiled=True)
    hidden = gated(arrived.reshape(-1, model_width), expert_gate[0], expert_up[0])
    expert_out = lax.psum_scatter(
        jnp.dot(hidden, expert_down[0], preferred_element_type=jnp.float32).astype(jnp.bfloat16),
        "tp",
        scatter_dimension=0,
        tiled=True,
    )
    returned = lax.all_to_all(
        expert_out.reshape(sp_size, capacity, model_width),
        "sp",
        split_axis=0,
        concat_axis=0,
        tiled=True,
    )
    picked = jnp.take(returned.reshape(-1, model_width), own_pos, axis=0)
    picked = picked.reshape(rows_dev, top_count, model_width)
    own_weights = lax.dynamic_slice_in_dim(route_weights, own_begin, rows_dev, 0)
    routed = jnp.sum(picked.astype(jnp.float32) * own_weights[:, :, None], axis=1)
    hidden = gated(normed, shared_gate, shared_up)
    shared = lax.psum_scatter(
        jnp.dot(hidden, shared_down, preferred_element_type=jnp.float32).astype(jnp.bfloat16),
        "tp",
        scatter_dimension=0,
        tiled=True,
    ).astype(jnp.float32)
    own_resid = lax.dynamic_slice_in_dim(residual, own_begin, rows_dev, 0).astype(jnp.float32)
    return (own_resid + routed + shared).astype(jnp.bfloat16)


def pool_kernel(rim_ref, pooled_ref, weight_ref, scale_ref, out_ref):
    tok_dev = pooled_ref.shape[0]
    window = lax.shift_left(jnp.int32(2), lax.axis_index("tp"))
    channels = pooled_ref[...].astype(jnp.float32)
    summed = jnp.concatenate([rim_ref[...].astype(jnp.float32), channels], 0)
    chosen, reach = summed, 1
    while reach < REACH:
        summed = summed + pltpu.roll(summed, reach, 0)
        reach *= 2
        chosen = jnp.where(window == reach, summed, chosen)
    position = lax.axis_index("sp") * tok_dev + lax.broadcasted_iota(jnp.int32, (tok_dev, 1), 0)
    counted = jnp.minimum(position + 1, window).astype(jnp.float32)
    pooled = (chosen[REACH:] / counted - channels).astype(jnp.bfloat16)
    mixed = jnp.dot(pooled, weight_ref[0], preferred_element_type=jnp.float32)
    out_ref[...] = (mixed * scale_ref[...]).astype(jnp.bfloat16)


def norm_kernel(
    grouped_ref, stream_ref, weight_ref, gain_ref, table_ref, packed_ref, resid_ref, wide_ref
):
    rows, width = resid_ref.shape
    tp_index = lax.axis_index("tp")
    own = pl.ds(pl.multiple_of(tp_index * rows, rows), rows)
    peer = pl.ds(pl.multiple_of((tp_index ^ X_BIT) * rows, rows), rows)

    def both(ref, cols=slice(None)):
        return jnp.concatenate([ref[own, cols], ref[peer, cols]], 0)

    grouped = both(grouped_ref)
    squares = jnp.zeros((2 * rows, 1), jnp.float32)
    block = min(512, width)
    for start in range(0, width, block):
        cols = slice(start, start + block)
        mixed = jnp.dot(grouped, weight_ref[:, cols], preferred_element_type=jnp.float32)
        residual = (both(stream_ref, cols).astype(jnp.float32) + mixed).astype(jnp.bfloat16)
        resid_ref[:, cols] = residual[:rows]
        wide = residual.astype(jnp.float32)
        wide_ref[:, cols] = wide
        squares = squares + jnp.sum(wide * wide, axis=1, keepdims=True)
    factor = lax.rsqrt(squares / width + EPSILON)
    for start in range(0, width, block):
        cols = slice(start, start + block)
        packed_ref[:, cols] = (wide_ref[:, cols] * factor * gain_ref[:, cols]).astype(jnp.bfloat16)
    packed_ref[:, width:] = both(table_ref)


def expert_kernel(n_pieces, n_outs, with_shared, *refs):
    pieces = refs[:n_pieces]
    weights = refs[n_pieces : n_pieces + (12 if with_shared else 6)]
    outs = refs[n_pieces + len(weights) :][:n_outs]
    rows_ref, scale_ref, hidden_ref, shared_ref = refs[-4:]
    width = outs[0].shape[1]
    experts = lax.axis_size("sp")
    mine = lax.axis_index("sp")
    begin = 0
    for piece in pieces:
        count = piece.shape[0]
        rows_ref[begin : begin + count] = piece[:, :width]
        marks = piece[:, width:].astype(jnp.float32)
        lane = lax.broadcasted_iota(jnp.int32, marks.shape, 1)
        named = (lane == mine) | (lane == mine + experts)
        scale_ref[begin : begin + count] = jnp.sum(
            jnp.where(named, marks, 0.0), axis=1, keepdims=True
        )
        begin += count

    def fill(target, gates, ups, block):
        column = 0
        for gate, up in zip(gates, ups):
            for start in range(0, gate.shape[1], block):
                cols = slice(start, start + block)
                a = jnp.dot(rows_ref[...], gate[:, cols], preferred_element_type=jnp.float32)
                b = jnp.dot(rows_ref[...], up[:, cols], preferred_element_type=jnp.float32)
                target[:, column : column + block] = (jax.nn.silu(a) * b).astype(jnp.bfloat16)
                column += block

    def product(source, downs, cols):
        total, column = None, 0
        for down in downs:
            depth = down.shape[0]
            part = jnp.dot(
                source[:, column : column + depth], down[:, cols],
                preferred_element_type=jnp.float32,
            )
            total = part if total is None else total + part
            column += depth
        return total

    fill(hidden_ref, weights[0:2], weights[2:4], 256)
    if with_shared:
        fill(shared_ref, weights[6:8], weights[8:10], 128)
    share = begin // n_outs
    block = min(512, width)
    for start in range(0, width, block):
        cols = slice(start, start + block)
        value = product(hidden_ref, weights[4:6], cols) * scale_ref[...]
        if with_shared:
            value = value + product(shared_ref, weights[10:12], cols)
        value = value.astype(jnp.bfloat16)
        for place, out in enumerate(outs):
            out[:, cols] = value[place * share : (place + 1) * share]


def in_vmem(count):
    return [pl.BlockSpec(memory_space=pltpu.VMEM)] * count


def run_expert(pieces, weights, n_outs, width):
    count = sum(piece.shape[0] for piece in pieces)
    with_shared = len(weights) == 12
    hidden = weights[0].shape[1] * 2
    shared = weights[6].shape[1] * 2 if with_shared else 128
    out = jax.ShapeDtypeStruct((count // n_outs, width), jnp.bfloat16)
    return pl.pallas_call(
        functools.partial(expert_kernel, len(pieces), n_outs, with_shared),
        out_shape=[out] * n_outs,
        in_specs=in_vmem(len(pieces) + len(weights)),
        out_specs=in_vmem(n_outs),
        scratch_shapes=[
            pltpu.VMEM((count, width), jnp.bfloat16),
            pltpu.VMEM((count, 1), jnp.float32),
            pltpu.VMEM((count, hidden), jnp.bfloat16),
            pltpu.VMEM((count, shared), jnp.bfloat16),
        ],
        compiler_params=pltpu.CompilerParams(vmem_limit_bytes=16 * MIB),
    )(*pieces, *weights)


def tied(*values):
    return lax.optimization_barrier(values)


def dense_plan(
    stream, pooled_in, pool_weight, pool_scale, out_weight, norm_gain, routes, route_weights,
    expert_gate, expert_up, expert_down, shared_gate, shared_up, shared_down,
):
    tok_dev, width = stream.shape
    tp_size = lax.axis_size("tp")
    sp_size = lax.axis_size("sp")
    rows = tok_dev // tp_size
    f32, bf16 = jnp.float32, jnp.bfloat16
    y_bit = tp_size
    z_bits = [2 * tp_size * k for k in range(sp_size // 2)]

    rim_rows = passed_along(pooled_in[tok_dev - REACH :], "sp", 1)
    weights = []
    for weight in (expert_gate[0], expert_up[0], expert_down[0]):
        weights += [weight, swapped(weight, CORE_BIT)]
    shared_weights = []
    for weight in (shared_gate, shared_up, shared_down):
        shared_weights += [weight, swapped(weight, CORE_BIT)]

    experts = jnp.arange(sp_size, dtype=jnp.int32)
    table = jnp.sum(
        jnp.where(routes[:, :, None] == experts, route_weights[:, :, None], 0.0), axis=1
    )
    high = lax.reduce_precision(table, 8, 7)
    table = jnp.concatenate([high, table - high], 1).astype(bf16)
    lanes = -(-2 * sp_size // 128) * 128
    table = jnp.pad(table, ((0, 0), (0, lanes - 2 * sp_size)))

    group_mix = pl.pallas_call(
        pool_kernel,
        out_shape=jax.ShapeDtypeStruct(pooled_in.shape, bf16),
        in_specs=in_vmem(4),
        out_specs=in_vmem(1)[0],
        compiler_params=pltpu.CompilerParams(vmem_limit_bytes=4 * MIB),
    )(rim_rows, pooled_in, pool_weight, pool_scale[None])
    grouped = lax.all_gather(group_mix, "tp", axis=1, tiled=True)
    pair, own_resid = pl.pallas_call(
        norm_kernel,
        out_shape=[
            jax.ShapeDtypeStruct((2 * rows, width + lanes), bf16),
            jax.ShapeDtypeStruct((rows, width), bf16),
        ],
        in_specs=in_vmem(5),
        out_specs=in_vmem(2),
        scratch_shapes=[pltpu.VMEM((2 * rows, width), f32)],
        compiler_params=pltpu.CompilerParams(vmem_limit_bytes=10 * MIB),
    )(grouped, stream, out_weight, norm_gain[None], table)

    kept, sent, got = {}, {}, {}
    z_1, z_2, _ = z_bits[1:]
    far_2 = swapped(pair[:rows], z_2)
    near = swapped(pair, y_bit)
    next_z = swapped(pair, z_1)
    (kept[0],) = run_expert([pair], weights + shared_weights, 1, width)
    far_2, kept[0] = tied(far_2, kept[0])
    far_3 = swapped(far_2, z_1)
    y_2 = swapped(far_2, y_bit)
    x_2 = swapped(far_2, X_BIT)
    near, far_2 = tied(near, far_2)
    (sent[0],) = run_expert([near], weights, 1, width)
    far_3, sent[0] = tied(far_3, sent[0])
    y_3 = swapped(far_3, y_bit)
    x_3 = swapped(far_3, X_BIT)
    y_2, far_3 = tied(y_2, far_3)
    xy_2 = swapped(y_2, X_BIT)
    next_z, y_2 = tied(next_z, y_2)
    y_1 = swapped(next_z, y_bit)
    sent[0], next_z = tied(sent[0], next_z)
    got[0] = swapped(sent[0], y_bit)
    y_3, next_z = tied(y_3, next_z)
    xy_3 = swapped(y_3, X_BIT)
    xy_2, y_3 = tied(xy_2, y_3)
    kept[2], sent[2] = run_expert([far_2, y_2, x_2, xy_2], weights, 2, width)
    got[2] = swapped(sent[2], X_BIT)
    xy_3, sent[2] = tied(xy_3, sent[2])
    kept[3], sent[3] = run_expert([far_3, y_3, x_3, xy_3], weights, 2, width)
    got[3] = swapped(sent[3], X_BIT)
    y_1, sent[3] = tied(y_1, sent[3])
    kept[1], sent[1] = run_expert([next_z, y_1], weights, 2, width)
    got[1] = swapped(sent[1], y_bit)

    def half(k, which):
        part = slice(which * rows, (which + 1) * rows)
        return kept[k][part].astype(f32) + got[k][part].astype(f32)

    more, flows = {}, {}
    for k in (2, 0, 3, 1):
        flip = X_BIT if k < 2 else y_bit
        more[k] = swapped(half(k, 1).astype(bf16), flip)
    for k in (2, 3, 1):
        flow = (half(k, 0) + more[k].astype(f32)).astype(bf16)
        flows[k] = swapped(flow, z_bits[k])
    result = half(0, 0) + more[0].astype(f32) + own_resid.astype(f32)
    for k in (2, 3, 1):
        result = result + flows[k].astype(f32)
    return result.astype(bf16)


def on_device(
    stream,
    pooled_in,
    pool_weight,
    pool_scale,
    out_weight,
    norm_gain,
    routes,
    route_weights,
    *experts,
):
    sp_size = lax.axis_size("sp")
    tp_size = lax.axis_size("tp")
    tok_dev = stream.shape[0]
    capacity = max(2, 2 * (tok_dev // tp_size) * routes.shape[1] // sp_size)
    crowded = 2 * sp_size * tp_size * capacity >= sp_size * tok_dev
    paired = tp_size == 4 and sp_size == 8
    pooling = (stream, pooled_in, pool_weight, pool_scale, out_weight, norm_gain)
    if crowded and paired:
        return dense_plan(*pooling, routes, route_weights, *experts)
    residual, normed = mixer(*pooling)
    return routed_plan(residual, normed, routes, route_weights, *experts)


def solution(mesh):
    placed = (
        P("sp", None),
        P("sp", "tp"),
        P("tp", None, None),
        P("tp"),
        P(),
        P(),
        P("sp", None),
        P("sp", None),
        P("sp", None, "tp"),
        P("sp", None, "tp"),
        P("sp", "tp", None),
        P(None, "tp"),
        P(None, "tp"),
        P("tp", None),
    )
    return jax.shard_map(
        on_device, mesh=mesh, in_specs=placed, out_specs=P(("sp", "tp"), None), check_vma=False
    )
```

profile of v0, /device:TPU:0, one launch (start us, length us, event | category | flops | bytes accessed | tf_op | source)
XLA Modules:
  0.0 143.9 jit_solution(9885964260245900063)
XLA Ops:
  0.0 0.5 collective-permute-start.2
  0.5 0.5 collective-permute-start.4
  1.0 0.7 slice.54
  1.7 4.9 %collective-permute-start = (bf16[16,256]{1,0:T(8,128)(2,1)S(1)}, bf16[16,256]{1,0:T(8,128)(2,1)S(1)}, u32[]{:S(2)}, u32[]{:S(2)}) collective-permute-start(bf16[16,256]{1,0:T(8,128)(2,1)S(1)} %slice.54), channel_id=1, source_target_pairs={{0,4},{4,8},{8,12},{12,16},{16,20},{20,24},{24,28},{1,5},{5,9},{9,... | collective-permute-start | bytes 24584 | tf_op jit(solution)/shard_map/ppermute | solution.py:24
  6.6 0.7 select_reduce_fusion
  7.3 0.6 collective-permute-done.rim_ref
  8.0 3.3 %collective-permute-done.5.refs_8_ = bf16[2048,128]{1,0:T(8,128)(2,1)S(1)} collective-permute-done((bf16[2048,128]{1,0:T(8,128)(2,1)}, bf16[2048,128]{1,0:T(8,128)(2,1)S(1)}, u32[]{:S(2)}, u32[]{:S(2)}) %collective-permute-start.5) | collective-permute-done | bytes 524320 | tf_op jit(solution)/shard_map/ppermute | solution.py:29
  11.2 0.4 collective-permute-start.7
  11.6 0.1 copy.20
  11.8 0.9 copy-done.8
  12.7 0.9 copy-done.9
  13.6 0.7 copy-done.11
  14.3 0.3 shard_map.136
  14.6 8.4 %all_gather.3.grouped_ref = bf16[256,1024]{1,0:T(8,128)(2,1)S(1)} all-gather(bf16[256,256]{1,0:T(8,128)(2,1)S(1)} %shard_map.136), channel_id=1, replica_groups=mesh['sp'=8,'tp'=4] {'tp'}, dimensions={1}, use_global_device_ids=true | all-gather | bytes 655360 | tf_op jit(solution)/shard_map/all_gather | solution.py:303
  23.0 2.2 %copy-done.3 = bf16[1024,2048]{1,0:T(8,128)(2,1)S(1)} copy-done((bf16[1024,2048]{1,0:T(8,128)(2,1)S(1)}, bf16[1024,2048]{1,0:T(8,128)(2,1)}, u32[]{:S(2)}) %copy-start.3) | copy-done | bytes 4194328
  25.2 1.2 copy-done.4
  26.4 0.7 copy-done.10
  27.1 1.0 shard_map.137
  28.1 1.7 %collective-permute-start.9 = (bf16[128,2176]{1,0:T(8,128)(2,1)S(1)}, bf16[128,2176]{1,0:T(8,128)(2,1)S(1)}, u32[]{:S(2)}, u32[]{:S(2)}) collective-permute-start(bf16[128,2176]{1,0:T(8,128)(2,1)S(1)} %get-tuple-element.31.refs_0_), channel_id=1, source_target_pairs={{0,4},{1,5},{2,6},{3,7},{4,0},{5,1},{6,2},{7,3},{8,12},{9,13},{10,... | collective-permute-start | bytes 1671176 | tf_op jit(solution)/shard_map/ppermute | solution.py:29
  29.9 2.6 %collective-permute-start.1 = (bf16[64,2176]{1,0:T(8,128)(2,1)S(1)}, bf16[64,2176]{1,0:T(8,128)(2,1)S(1)}, u32[]{:S(2)}, u32[]{:S(2)}) collective-permute-start(bf16[64,2176]{1,0:T(8,128)(2,1)S(1)} %slice.55), channel_id=1, source_target_pairs={{0,16},{1,17},{2,18},{3,19},{4,20},{5,21},{6,22},{7,23},{8,24},{9,... | collective-permute-start | bytes 835592 | tf_op jit(solution)/shard_map/ppermute | solution.py:29
  32.5 1.6 %collective-permute-start.10 = (bf16[128,2176]{1,0:T(8,128)(2,1)S(1)}, bf16[128,2176]{1,0:T(8,128)(2,1)S(1)}, u32[]{:S(2)}, u32[]{:S(2)}) collective-permute-start(bf16[128,2176]{1,0:T(8,128)(2,1)S(1)} %get-tuple-element.31.refs_0_), channel_id=1, source_target_pairs={{0,8},{1,9},{2,10},{3,11},{4,12},{5,13},{6,14},{7,15},{8,0},{9,1},... | collective-permute-start | bytes 1671176 | tf_op jit(solution)/shard_map/ppermute | solution.py:29
  34.1 1.0 copy-done.7
  35.1 4.9 %shard_map.138 = bf16[128,2048]{1,0:T(8,128)(2,1)S(1)} custom-call(bf16[128,2176]{1,0:T(8,128)(2,1)S(1)} %get-tuple-element.31.refs_0_, bf16[2048,512]{1,0:T(8,128)(2,1)S(1)} %bitcast.6, bf16[2048,512]{1,0:T(8,128)(2,1)S(1)} %collective-permute-done.2.refs_2_.refs_5_.refs_3_, bf16[2048,512]{1,0:T(8,128)(2,1)S(1)} %bitcast.12, ...), custom_call_target="tpu_custom_call" | custom-call | tf_op jit(solution)/shard_map/pallas_call | solution.py:248
  40.1 5.4 %collective-permute-done.1.refs_0_ = bf16[64,2176]{1,0:T(8,128)(2,1)S(1)} collective-permute-done((bf16[64,2176]{1,0:T(8,128)(2,1)S(1)}, bf16[64,2176]{1,0:T(8,128)(2,1)S(1)}, u32[]{:S(2)}, u32[]{:S(2)}) %collective-permute-start.1) | collective-permute-done | bytes 278560 | tf_op jit(solution)/shard_map/ppermute | solution.py:29
  45.5 0.6 collective-permute-start.8
  46.1 0.5 collective-permute-start.11
  46.6 4.1 %shard_map.139 = bf16[128,2048]{1,0:T(8,128)(2,1)S(1)} custom-call(bf16[128,2176]{1,0:T(8,128)(2,1)S(1)} %collective-permute-done.9.refs_0_, bf16[2048,512]{1,0:T(8,128)(2,1)S(1)} %bitcast.7, bf16[2048,512]{1,0:T(8,128)(2,1)S(1)} %collective-permute-done.2.refs_2_.refs_5_.refs_3_, bf16[2048,512]{1,0:T(8,128)(2,1)S(1)} %bitcast.13, ...), custom_call_target="tpu_custom_call" | custom-call | tf_op jit(solution)/shard_map/pallas_call | solution.py:248
  50.7 6.9 %collective-permute-done.8.refs_0_ = bf16[64,2176]{1,0:T(8,128)(2,1)S(1)} collective-permute-done((bf16[64,2176]{1,0:T(8,128)(2,1)S(1)}, bf16[64,2176]{1,0:T(8,128)(2,1)S(1)}, u32[]{:S(2)}, u32[]{:S(2)}) %collective-permute-start.8) | collective-permute-done | bytes 278560 | tf_op jit(solution)/shard_map/ppermute | solution.py:29
  57.6 0.5 collective-permute-start.16
  58.1 1.5 %collective-permute-start.15 = (bf16[64,2176]{1,0:T(8,128)(2,1)S(1)}, bf16[64,2176]{1,0:T(8,128)(2,1)S(1)}, u32[]{:S(2)}, u32[]{:S(2)}) collective-permute-start(bf16[64,2176]{1,0:T(8,128)(2,1)S(1)} %collective-permute-done.11.refs_1_), channel_id=1, source_target_pairs={{0,2},{1,3},{2,0},{3,1},{4,6},{5,7},{6,4},{7,5},{8,10},{9,11},{10,... | collective-permute-start | bytes 835592 | tf_op jit(solution)/shard_map/ppermute | solution.py:29
  59.6 0.5 collective-permute-start.14
  60.1 5.0 %collective-permute-done.16.refs_1_ = bf16[64,2176]{1,0:T(8,128)(2,1)S(1)} collective-permute-done((bf16[64,2176]{1,0:T(8,128)(2,1)S(1)}, bf16[64,2176]{1,0:T(8,128)(2,1)S(1)}, u32[]{:S(2)}, u32[]{:S(2)}) %collective-permute-start.16) | collective-permute-done | bytes 278560 | tf_op jit(solution)/shard_map/ppermute | solution.py:29
  65.1 2.5 %collective-permute-done.15.refs_3_ = bf16[64,2176]{1,0:T(8,128)(2,1)S(1)} collective-permute-done((bf16[64,2176]{1,0:T(8,128)(2,1)S(1)}, bf16[64,2176]{1,0:T(8,128)(2,1)S(1)}, u32[]{:S(2)}, u32[]{:S(2)}) %collective-permute-start.15) | collective-permute-done | bytes 278560 | tf_op jit(solution)/shard_map/ppermute | solution.py:29
  67.6 3.7 %collective-permute-done.14.refs_2_ = bf16[64,2176]{1,0:T(8,128)(2,1)S(1)} collective-permute-done((bf16[64,2176]{1,0:T(8,128)(2,1)S(1)}, bf16[64,2176]{1,0:T(8,128)(2,1)S(1)}, u32[]{:S(2)}, u32[]{:S(2)}) %collective-permute-start.14) | collective-permute-done | bytes 278560 | tf_op jit(solution)/shard_map/ppermute | solution.py:29
  71.3 5.7 %shard_map.140 = (bf16[128,2048]{1,0:T(8,128)(2,1)S(1)}, bf16[128,2048]{1,0:T(8,128)(2,1)S(1)}) custom-call(bf16[64,2176]{1,0:T(8,128)(2,1)S(1)} %collective-permute-done.1.refs_0_, bf16[64,2176]{1,0:T(8,128)(2,1)S(1)} %collective-permute-done.11.refs_1_, bf16[64,2176]{1,0:T(8,128)(2,1)S(1)} %collective-permute-done.14.refs_2_, ...), custom_call_target="tpu_custom_call" | custom-call | tf_op jit(solution)/shard_map/pallas_call | solution.py:248
  77.0 1.6 %collective-permute-start.17 = (bf16[128,2048]{1,0:T(8,128)(2,1)S(1)}, bf16[128,2048]{1,0:T(8,128)(2,1)S(1)}, u32[]{:S(2)}, u32[]{:S(2)}) collective-permute-start(bf16[128,2048]{1,0:T(8,128)(2,1)S(1)} %get-tuple-element.47), channel_id=1, source_target_pairs={{0,2},{1,3},{2,0},{3,1},{4,6},{5,7},{6,4},{7,5},{8,10},{9,11},{10,... | collective-permute-start | bytes 1572872 | tf_op jit(solution)/shard_map/ppermute | solution.py:29
  78.5 0.5 collective-permute-start.21
  79.0 1.5 %collective-permute-start.20 = (bf16[64,2176]{1,0:T(8,128)(2,1)S(1)}, bf16[64,2176]{1,0:T(8,128)(2,1)S(1)}, u32[]{:S(2)}, u32[]{:S(2)}) collective-permute-start(bf16[64,2176]{1,0:T(8,128)(2,1)S(1)} %collective-permute-done.8.refs_0_), channel_id=1, source_target_pairs={{0,2},{1,3},{2,0},{3,1},{4,6},{5,7},{6,4},{7,5},{8,10},{9,11},{10,... | collective-permute-start | bytes 835592 | tf_op jit(solution)/shard_map/ppermute | solution.py:29
  80.6 1.5 %collective-permute-start.12 = (bf16[128,2048]{1,0:T(8,128)(2,1)S(1)}, bf16[128,2048]{1,0:T(8,128)(2,1)S(1)}, u32[]{:S(2)}, u32[]{:S(2)}) collective-permute-start(bf16[128,2048]{1,0:T(8,128)(2,1)S(1)} %shard_map.139), channel_id=1, source_target_pairs={{0,4},{1,5},{2,6},{3,7},{4,0},{5,1},{6,2},{7,3},{8,12},{9,13},{10,... | collective-permute-start | bytes 1572872 | tf_op jit(solution)/shard_map/ppermute | solution.py:29
  82.1 0.5 collective-permute-start.25
  82.6 15.0 %collective-permute-done.21.refs_3_ = bf16[64,2176]{1,0:T(8,128)(2,1)S(1)} collective-permute-done((bf16[64,2176]{1,0:T(8,128)(2,1)S(1)}, bf16[64,2176]{1,0:T(8,128)(2,1)S(1)}, u32[]{:S(2)}, u32[]{:S(2)}) %collective-permute-start.21) | collective-permute-done | bytes 278560 | tf_op jit(solution)/shard_map/ppermute | solution.py:29
  97.6 3.0 %collective-permute-done.20.refs_2_ = bf16[64,2176]{1,0:T(8,128)(2,1)S(1)} collective-permute-done((bf16[64,2176]{1,0:T(8,128)(2,1)S(1)}, bf16[64,2176]{1,0:T(8,128)(2,1)S(1)}, u32[]{:S(2)}, u32[]{:S(2)}) %collective-permute-start.20) | collective-permute-done | bytes 278560 | tf_op jit(solution)/shard_map/ppermute | solution.py:29
  100.6 5.7 %shard_map.141 = (bf16[128,2048]{1,0:T(8,128)(2,1)S(1)}, bf16[128,2048]{1,0:T(8,128)(2,1)S(1)}) custom-call(bf16[64,2176]{1,0:T(8,128)(2,1)S(1)} %collective-permute-done.8.refs_0_, bf16[64,2176]{1,0:T(8,128)(2,1)S(1)} %collective-permute-done.16.refs_1_, bf16[64,2176]{1,0:T(8,128)(2,1)S(1)} %collective-permute-done.20.refs_2_, ...), custom_call_target="tpu_custom_call" | custom-call | tf_op jit(solution)/shard_map/pallas_call | solution.py:248
  106.3 1.6 %collective-permute-start.22 = (bf16[128,2048]{1,0:T(8,128)(2,1)S(1)}, bf16[128,2048]{1,0:T(8,128)(2,1)S(1)}, u32[]{:S(2)}, u32[]{:S(2)}) collective-permute-start(bf16[128,2048]{1,0:T(8,128)(2,1)S(1)} %get-tuple-element.52), channel_id=1, source_target_pairs={{0,2},{1,3},{2,0},{3,1},{4,6},{5,7},{6,4},{7,5},{8,10},{9,11},{10,... | collective-permute-start | bytes 1572872 | tf_op jit(solution)/shard_map/ppermute | solution.py:29
  107.9 1.6 %collective-permute-start.18 = (bf16[64,2048]{1,0:T(8,128)(2,1)S(1)}, bf16[64,2048]{1,0:T(8,128)(2,1)S(1)}, u32[]{:S(2)}, u32[]{:S(2)}) collective-permute-start(bf16[64,2048]{1,0:T(8,128)(2,1)S(1)} %add_convert_fusion.6), channel_id=1, source_target_pairs={{0,4},{1,5},{2,6},{3,7},{4,0},{5,1},{6,2},{7,3},{8,12},{9,13},{10,... | collective-permute-start | bytes 786440 | tf_op jit(solution)/shard_map/ppermute | solution.py:29
  109.5 0.2 add_convert_fusion.7
  109.8 0.6 collective-permute-start.13
  110.4 5.7 %shard_map.142 = (bf16[128,2048]{1,0:T(8,128)(2,1)S(1)}, bf16[128,2048]{1,0:T(8,128)(2,1)S(1)}) custom-call(bf16[128,2176]{1,0:T(8,128)(2,1)S(1)} %collective-permute-done.10.refs_0_, bf16[128,2176]{1,0:T(8,128)(2,1)S(1)} %collective-permute-done.25.refs_1_, bf16[2048,512]{1,0:T(8,128)(2,1)S(1)} %bitcast.10, ...), custom_call_target="tpu_custom_call" | custom-call | tf_op jit(solution)/shard_map/pallas_call | solution.py:248
  116.1 0.5 collective-permute-start.26
  116.6 0.1 add_convert_fusion.5
  116.7 2.0 %collective-permute-start.19 = (bf16[64,2048]{1,0:T(8,128)(2,1)S(1)}, bf16[64,2048]{1,0:T(8,128)(2,1)S(1)}, u32[]{:S(2)}, u32[]{:S(2)}) collective-permute-start(bf16[64,2048]{1,0:T(8,128)(2,1)S(1)} %add_convert_fusion.5), channel_id=1, source_target_pairs={{0,16},{1,17},{2,18},{3,19},{4,20},{5,21},{6,22},{7,23},{8,24},{9,... | collective-permute-start | bytes 786440 | tf_op jit(solution)/shard_map/ppermute | solution.py:29
  118.7 1.2 collective-permute-done.22
  120.0 1.6 %collective-permute-start.23 = (bf16[64,2048]{1,0:T(8,128)(2,1)S(1)}, bf16[64,2048]{1,0:T(8,128)(2,1)S(1)}, u32[]{:S(2)}, u32[]{:S(2)}) collective-permute-start(bf16[64,2048]{1,0:T(8,128)(2,1)S(1)} %add_convert_fusion.4), channel_id=1, source_target_pairs={{0,4},{1,5},{2,6},{3,7},{4,0},{5,1},{6,2},{7,3},{8,12},{9,13},{10,... | collective-permute-start | bytes 786440 | tf_op jit(solution)/shard_map/ppermute | solution.py:29
  121.6 7.3 %collective-permute-done.26 = bf16[128,2048]{1,0:T(8,128)(2,1)S(1)} collective-permute-done((bf16[128,2048]{1,0:T(8,128)(2,1)S(1)}, bf16[128,2048]{1,0:T(8,128)(2,1)S(1)}, u32[]{:S(2)}, u32[]{:S(2)}) %collective-permute-start.26) | collective-permute-done | bytes 524320 | tf_op jit(solution)/shard_map/ppermute | solution.py:29
  129.0 1.6 %collective-permute-start.27 = (bf16[64,2048]{1,0:T(8,128)(2,1)S(1)}, bf16[64,2048]{1,0:T(8,128)(2,1)S(1)}, u32[]{:S(2)}, u32[]{:S(2)}) collective-permute-start(bf16[64,2048]{1,0:T(8,128)(2,1)S(1)} %add_convert_fusion.2), channel_id=1, source_target_pairs={{0,2},{1,3},{2,0},{3,1},{4,6},{5,7},{6,4},{7,5},{8,10},{9,11},{10,... | collective-permute-start | bytes 786440 | tf_op jit(solution)/shard_map/ppermute | solution.py:29
  130.5 1.2 collective-permute-done.23
  131.7 0.1 add_convert_fusion.3
  131.8 2.7 %collective-permute-start.24 = (bf16[64,2048]{1,0:T(8,128)(2,1)S(1)}, bf16[64,2048]{1,0:T(8,128)(2,1)S(1)}, u32[]{:S(2)}, u32[]{:S(2)}) collective-permute-start(bf16[64,2048]{1,0:T(8,128)(2,1)S(1)} %add_convert_fusion.3), channel_id=1, source_target_pairs={{0,24},{1,25},{2,26},{3,27},{4,28},{5,29},{6,30},{7,31},{8,16},{9,... | collective-permute-start | bytes 786440 | tf_op jit(solution)/shard_map/ppermute | solution.py:29
  134.5 0.9 collective-permute-done.27
  135.4 0.1 add_convert_fusion.1
  135.5 2.3 %collective-permute-start.28 = (bf16[64,2048]{1,0:T(8,128)(2,1)S(1)}, bf16[64,2048]{1,0:T(8,128)(2,1)S(1)}, u32[]{:S(2)}, u32[]{:S(2)}) collective-permute-start(bf16[64,2048]{1,0:T(8,128)(2,1)S(1)} %add_convert_fusion.1), channel_id=1, source_target_pairs={{0,8},{1,9},{2,10},{3,11},{4,12},{5,13},{6,14},{7,15},{8,0},{9,1},... | collective-permute-start | bytes 786440 | tf_op jit(solution)/shard_map/ppermute | solution.py:29
  137.8 2.4 %collective-permute-done.24 = bf16[64,2048]{1,0:T(8,128)(2,1)S(1)} collective-permute-done((bf16[64,2048]{1,0:T(8,128)(2,1)S(1)}, bf16[64,2048]{1,0:T(8,128)(2,1)S(1)}, u32[]{:S(2)}, u32[]{:S(2)}) %collective-permute-start.24) | collective-permute-done | bytes 262176 | tf_op jit(solution)/shard_map/ppermute | solution.py:29
  140.2 2.7 %collective-permute-done.28 = bf16[64,2048]{1,0:T(8,128)(2,1)S(1)} collective-permute-done((bf16[64,2048]{1,0:T(8,128)(2,1)S(1)}, bf16[64,2048]{1,0:T(8,128)(2,1)S(1)}, u32[]{:S(2)}, u32[]{:S(2)}) %collective-permute-start.28) | collective-permute-done | bytes 262176 | tf_op jit(solution)/shard_map/ppermute | solution.py:29
  143.0 1.0 add_convert_fusion
  (41 shorter events, 0.4 us)
Async XLA Ops:
  0.0 32.5 %collective-permute-start.2 = (bf16[2048,512]{1,0:T(8,128)(2,1)}, bf16[2048,512]{1,0:T(8,128)(2,1)S(1)}, u32[]{:S(2)}, u32[]{:S(2)}) collective-permute-start(bf16[2048,512]{1,0:T(8,128)(2,1)} %bitcast.5), channel_id=1, source_target_pairs={{0,1},{1,0},{2,3},{3,2},{4,5},{5,4},{6,7},{7,6},{8,9},{9,8},{10,11... | collective-permute-start | bytes 6291464 | tf_op jit(solution)/shard_map/ppermute | solution.py:29
  0.5 33.5 %collective-permute-start.3 = (bf16[2048,512]{1,0:T(8,128)(2,1)}, bf16[2048,512]{1,0:T(8,128)(2,1)}, u32[]{:S(2)}, u32[]{:S(2)}) collective-permute-start(bf16[2048,512]{1,0:T(8,128)(2,1)} %bitcast.11), channel_id=1, source_target_pairs={{0,1},{1,0},{2,3},{3,2},{4,5},{5,4},{6,7},{7,6},{8,9},{9,8},{10,11... | collective-permute-start | bytes 6291464 | tf_op jit(solution)/shard_map/ppermute | solution.py:29
  0.5 33.5 %collective-permute-start.4 = (bf16[512,2048]{1,0:T(8,128)(2,1)}, bf16[512,2048]{1,0:T(8,128)(2,1)}, u32[]{:S(2)}, u32[]{:S(2)}) collective-permute-start(bf16[512,2048]{1,0:T(8,128)(2,1)} %bitcast.17), channel_id=1, source_target_pairs={{0,1},{1,0},{2,3},{3,2},{4,5},{5,4},{6,7},{7,6},{8,9},{9,8},{10,11... | collective-permute-start | bytes 6291464 | tf_op jit(solution)/shard_map/ppermute | solution.py:29
  1.0 10.2 %collective-permute-start.5 = (bf16[2048,128]{1,0:T(8,128)(2,1)}, bf16[2048,128]{1,0:T(8,128)(2,1)S(1)}, u32[]{:S(2)}, u32[]{:S(2)}) collective-permute-start(bf16[2048,128]{1,0:T(8,128)(2,1)} %refs_7_.1), channel_id=1, source_target_pairs={{0,1},{1,0},{2,3},{3,2},{4,5},{5,4},{6,7},{7,6},{8,9},{9,8},{10,11... | collective-permute-start | bytes 1572872 | tf_op jit(solution)/shard_map/ppermute | solution.py:29
  1.7 6.2 %collective-permute-start = (bf16[16,256]{1,0:T(8,128)(2,1)S(1)}, bf16[16,256]{1,0:T(8,128)(2,1)S(1)}, u32[]{:S(2)}, u32[]{:S(2)}) collective-permute-start(bf16[16,256]{1,0:T(8,128)(2,1)S(1)} %slice.54), channel_id=1, source_target_pairs={{0,4},{4,8},{8,12},{12,16},{16,20},{20,24},{24,28},{1,5},{5,9},{9,... | collective-permute-start | bytes 24584 | tf_op jit(solution)/shard_map/ppermute | solution.py:24
  8.0 20.2 %collective-permute-start.6 = (bf16[2048,128]{1,0:T(8,128)(2,1)}, bf16[2048,128]{1,0:T(8,128)(2,1)S(1)}, u32[]{:S(2)}, u32[]{:S(2)}) collective-permute-start(bf16[2048,128]{1,0:T(8,128)(2,1)} %refs_9_.1), channel_id=1, source_target_pairs={{0,1},{1,0},{2,3},{3,2},{4,5},{5,4},{6,7},{7,6},{8,9},{9,8},{10,11... | collective-permute-start | bytes 1572872 | tf_op jit(solution)/shard_map/ppermute | solution.py:29
  11.2 18.6 %collective-permute-start.7 = (bf16[128,2048]{1,0:T(8,128)(2,1)}, bf16[128,2048]{1,0:T(8,128)(2,1)}, u32[]{:S(2)}, u32[]{:S(2)}) collective-permute-start(bf16[128,2048]{1,0:T(8,128)(2,1)} %refs_11_.1), channel_id=1, source_target_pairs={{0,1},{1,0},{2,3},{3,2},{4,5},{5,4},{6,7},{7,6},{8,9},{9,8},{10,11... | collective-permute-start | bytes 1572872 | tf_op jit(solution)/shard_map/ppermute | solution.py:29
  11.8 0.9 copy-start.8
  12.7 0.9 copy-start.9
  13.6 0.7 copy-start.11
  14.3 19.8 %copy-start.6 = (bf16[2048,128]{1,0:T(8,128)(2,1)S(1)}, bf16[2048,128]{1,0:T(8,128)(2,1)}, u32[]{:S(2)}) copy-start(bf16[2048,128]{1,0:T(8,128)(2,1)} %refs_9_.1) | copy-start | bytes 1572868
  14.6 19.4 %copy-start.5 = (bf16[2048,128]{1,0:T(8,128)(2,1)S(1)}, bf16[2048,128]{1,0:T(8,128)(2,1)}, u32[]{:S(2)}) copy-start(bf16[2048,128]{1,0:T(8,128)(2,1)} %refs_7_.1) | copy-start | bytes 1572868
  23.0 2.2 %copy-start.3 = (bf16[1024,2048]{1,0:T(8,128)(2,1)S(1)}, bf16[1024,2048]{1,0:T(8,128)(2,1)}, u32[]{:S(2)}) copy-start(bf16[1024,2048]{1,0:T(8,128)(2,1)} %weight_ref.3) | copy-start | bytes 12582916
  25.2 1.2 copy-start.4
  26.4 0.7 copy-start.10
  27.1 6.9 %copy-start = (bf16[1,2048,512]{2,1,0:T(8,128)(2,1)S(1)}, bf16[1,2048,512]{2,1,0:T(8,128)(2,1)}, u32[]{:S(2)}) copy-start(bf16[1,2048,512]{2,1,0:T(8,128)(2,1)} %param.22) | copy-start | bytes 6291460
  27.1 6.9 %copy-start.1 = (bf16[1,2048,512]{2,1,0:T(8,128)(2,1)S(1)}, bf16[1,2048,512]{2,1,0:T(8,128)(2,1)}, u32[]{:S(2)}) copy-start(bf16[1,2048,512]{2,1,0:T(8,128)(2,1)} %param.23) | copy-start | bytes 6291460
  27.1 6.9 %copy-start.2 = (bf16[1,512,2048]{2,1,0:T(8,128)(2,1)S(1)}, bf16[1,512,2048]{2,1,0:T(8,128)(2,1)}, u32[]{:S(2)}) copy-start(bf16[1,512,2048]{2,1,0:T(8,128)(2,1)} %param.24) | copy-start | bytes 6291460
  28.1 18.5 %collective-permute-start.9 = (bf16[128,2176]{1,0:T(8,128)(2,1)S(1)}, bf16[128,2176]{1,0:T(8,128)(2,1)S(1)}, u32[]{:S(2)}, u32[]{:S(2)}) collective-permute-start(bf16[128,2176]{1,0:T(8,128)(2,1)S(1)} %get-tuple-element.31.refs_0_), channel_id=1, source_target_pairs={{0,4},{1,5},{2,6},{3,7},{4,0},{5,1},{6,2},{7,3},{8,12},{9,13},{10,... | collective-permute-start | bytes 1671176 | tf_op jit(solution)/shard_map/ppermute | solution.py:29
  29.9 15.6 %collective-permute-start.1 = (bf16[64,2176]{1,0:T(8,128)(2,1)S(1)}, bf16[64,2176]{1,0:T(8,128)(2,1)S(1)}, u32[]{:S(2)}, u32[]{:S(2)}) collective-permute-start(bf16[64,2176]{1,0:T(8,128)(2,1)S(1)} %slice.55), channel_id=1, source_target_pairs={{0,16},{1,17},{2,18},{3,19},{4,20},{5,21},{6,22},{7,23},{8,24},{9,... | collective-permute-start | bytes 835592 | tf_op jit(solution)/shard_map/ppermute | solution.py:29
  32.5 27.6 %collective-permute-start.10 = (bf16[128,2176]{1,0:T(8,128)(2,1)S(1)}, bf16[128,2176]{1,0:T(8,128)(2,1)S(1)}, u32[]{:S(2)}, u32[]{:S(2)}) collective-permute-start(bf16[128,2176]{1,0:T(8,128)(2,1)S(1)} %get-tuple-element.31.refs_0_), channel_id=1, source_target_pairs={{0,8},{1,9},{2,10},{3,11},{4,12},{5,13},{6,14},{7,15},{8,0},{9,1},... | collective-permute-start | bytes 1671176 | tf_op jit(solution)/shard_map/ppermute | solution.py:29
  34.1 1.0 copy-start.7
  45.5 12.1 %collective-permute-start.8 = (bf16[64,2176]{1,0:T(8,128)(2,1)S(1)}, bf16[64,2176]{1,0:T(8,128)(2,1)S(1)}, u32[]{:S(2)}, u32[]{:S(2)}) collective-permute-start(bf16[64,2176]{1,0:T(8,128)(2,1)S(1)} %collective-permute-done.1.refs_0_), channel_id=1, source_target_pairs={{0,8},{1,9},{2,10},{3,11},{4,12},{5,13},{6,14},{7,15},{8,0},{9,1},... | collective-permute-start | bytes 835592 | tf_op jit(solution)/shard_map/ppermute | solution.py:29
  46.1 12.0 %collective-permute-start.11 = (bf16[64,2176]{1,0:T(8,128)(2,1)S(1)}, bf16[64,2176]{1,0:T(8,128)(2,1)S(1)}, u32[]{:S(2)}, u32[]{:S(2)}) collective-permute-start(bf16[64,2176]{1,0:T(8,128)(2,1)S(1)} %collective-permute-done.1.refs_0_), channel_id=1, source_target_pairs={{0,4},{1,5},{2,6},{3,7},{4,0},{5,1},{6,2},{7,3},{8,12},{9,13},{10,... | collective-permute-start | bytes 835592 | tf_op jit(solution)/shard_map/ppermute | solution.py:29
  57.6 7.5 %collective-permute-start.16 = (bf16[64,2176]{1,0:T(8,128)(2,1)S(1)}, bf16[64,2176]{1,0:T(8,128)(2,1)S(1)}, u32[]{:S(2)}, u32[]{:S(2)}) collective-permute-start(bf16[64,2176]{1,0:T(8,128)(2,1)S(1)} %collective-permute-done.8.refs_0_), channel_id=1, source_target_pairs={{0,4},{1,5},{2,6},{3,7},{4,0},{5,1},{6,2},{7,3},{8,12},{9,13},{10,... | collective-permute-start | bytes 835592 | tf_op jit(solution)/shard_map/ppermute | solution.py:29
  58.1 9.5 %collective-permute-start.15 = (bf16[64,2176]{1,0:T(8,128)(2,1)S(1)}, bf16[64,2176]{1,0:T(8,128)(2,1)S(1)}, u32[]{:S(2)}, u32[]{:S(2)}) collective-permute-start(bf16[64,2176]{1,0:T(8,128)(2,1)S(1)} %collective-permute-done.11.refs_1_), channel_id=1, source_target_pairs={{0,2},{1,3},{2,0},{3,1},{4,6},{5,7},{6,4},{7,5},{8,10},{9,11},{10,... | collective-permute-start | bytes 835592 | tf_op jit(solution)/shard_map/ppermute | solution.py:29
  59.6 11.6 %collective-permute-start.14 = (bf16[64,2176]{1,0:T(8,128)(2,1)S(1)}, bf16[64,2176]{1,0:T(8,128)(2,1)S(1)}, u32[]{:S(2)}, u32[]{:S(2)}) collective-permute-start(bf16[64,2176]{1,0:T(8,128)(2,1)S(1)} %collective-permute-done.1.refs_0_), channel_id=1, source_target_pairs={{0,2},{1,3},{2,0},{3,1},{4,6},{5,7},{6,4},{7,5},{8,10},{9,11},{10,... | collective-permute-start | bytes 835592 | tf_op jit(solution)/shard_map/ppermute | solution.py:29
  77.0 30.9 %collective-permute-start.17 = (bf16[128,2048]{1,0:T(8,128)(2,1)S(1)}, bf16[128,2048]{1,0:T(8,128)(2,1)S(1)}, u32[]{:S(2)}, u32[]{:S(2)}) collective-permute-start(bf16[128,2048]{1,0:T(8,128)(2,1)S(1)} %get-tuple-element.47), channel_id=1, source_target_pairs={{0,2},{1,3},{2,0},{3,1},{4,6},{5,7},{6,4},{7,5},{8,10},{9,11},{10,... | collective-permute-start | bytes 1572872 | tf_op jit(solution)/shard_map/ppermute | solution.py:29
  78.5 19.1 %collective-permute-start.21 = (bf16[64,2176]{1,0:T(8,128)(2,1)S(1)}, bf16[64,2176]{1,0:T(8,128)(2,1)S(1)}, u32[]{:S(2)}, u32[]{:S(2)}) collective-permute-start(bf16[64,2176]{1,0:T(8,128)(2,1)S(1)} %collective-permute-done.16.refs_1_), channel_id=1, source_target_pairs={{0,2},{1,3},{2,0},{3,1},{4,6},{5,7},{6,4},{7,5},{8,10},{9,11},{10,... | collective-permute-start | bytes 835592 | tf_op jit(solution)/shard_map/ppermute | solution.py:29
  79.0 21.5 %collective-permute-start.20 = (bf16[64,2176]{1,0:T(8,128)(2,1)S(1)}, bf16[64,2176]{1,0:T(8,128)(2,1)S(1)}, u32[]{:S(2)}, u32[]{:S(2)}) collective-permute-start(bf16[64,2176]{1,0:T(8,128)(2,1)S(1)} %collective-permute-done.8.refs_0_), channel_id=1, source_target_pairs={{0,2},{1,3},{2,0},{3,1},{4,6},{5,7},{6,4},{7,5},{8,10},{9,11},{10,... | collective-permute-start | bytes 835592 | tf_op jit(solution)/shard_map/ppermute | solution.py:29
  80.6 29.0 %collective-permute-start.12 = (bf16[128,2048]{1,0:T(8,128)(2,1)S(1)}, bf16[128,2048]{1,0:T(8,128)(2,1)S(1)}, u32[]{:S(2)}, u32[]{:S(2)}) collective-permute-start(bf16[128,2048]{1,0:T(8,128)(2,1)S(1)} %shard_map.139), channel_id=1, source_target_pairs={{0,4},{1,5},{2,6},{3,7},{4,0},{5,1},{6,2},{7,3},{8,12},{9,13},{10,... | collective-permute-start | bytes 1572872 | tf_op jit(solution)/shard_map/ppermute | solution.py:29
  82.1 28.3 %collective-permute-start.25 = (bf16[128,2176]{1,0:T(8,128)(2,1)S(1)}, bf16[128,2176]{1,0:T(8,128)(2,1)S(1)}, u32[]{:S(2)}, u32[]{:S(2)}) collective-permute-start(bf16[128,2176]{1,0:T(8,128)(2,1)S(1)} %collective-permute-done.10.refs_0_), channel_id=1, source_target_pairs={{0,4},{1,5},{2,6},{3,7},{4,0},{5,1},{6,2},{7,3},{8,12},{9,13},{10,... | collective-permute-start | bytes 1671176 | tf_op jit(solution)/shard_map/ppermute | solution.py:29
  106.3 13.7 %collective-permute-start.22 = (bf16[128,2048]{1,0:T(8,128)(2,1)S(1)}, bf16[128,2048]{1,0:T(8,128)(2,1)S(1)}, u32[]{:S(2)}, u32[]{:S(2)}) collective-permute-start(bf16[128,2048]{1,0:T(8,128)(2,1)S(1)} %get-tuple-element.52), channel_id=1, source_target_pairs={{0,2},{1,3},{2,0},{3,1},{4,6},{5,7},{6,4},{7,5},{8,10},{9,11},{10,... | collective-permute-start | bytes 1572872 | tf_op jit(solution)/shard_map/ppermute | solution.py:29
  107.9 8.7 %collective-permute-start.18 = (bf16[64,2048]{1,0:T(8,128)(2,1)S(1)}, bf16[64,2048]{1,0:T(8,128)(2,1)S(1)}, u32[]{:S(2)}, u32[]{:S(2)}) collective-permute-start(bf16[64,2048]{1,0:T(8,128)(2,1)S(1)} %add_convert_fusion.6), channel_id=1, source_target_pairs={{0,4},{1,5},{2,6},{3,7},{4,0},{5,1},{6,2},{7,3},{8,12},{9,13},{10,... | collective-permute-start | bytes 786440 | tf_op jit(solution)/shard_map/ppermute | solution.py:29
  109.8 28.1 %collective-permute-start.13 = (bf16[64,2048]{1,0:T(8,128)(2,1)S(1)}, bf16[64,2048]{1,0:T(8,128)(2,1)S(1)}, u32[]{:S(2)}, u32[]{:S(2)}) collective-permute-start(bf16[64,2048]{1,0:T(8,128)(2,1)S(1)} %add_convert_fusion.7), channel_id=1, source_target_pairs={{0,2},{1,3},{2,0},{3,1},{4,6},{5,7},{6,4},{7,5},{8,10},{9,11},{10,... | collective-permute-start | bytes 786440 | tf_op jit(solution)/shard_map/ppermute | solution.py:29
  116.1 12.8 %collective-permute-start.26 = (bf16[128,2048]{1,0:T(8,128)(2,1)S(1)}, bf16[128,2048]{1,0:T(8,128)(2,1)S(1)}, u32[]{:S(2)}, u32[]{:S(2)}) collective-permute-start(bf16[128,2048]{1,0:T(8,128)(2,1)S(1)} %get-tuple-element.56), channel_id=1, source_target_pairs={{0,4},{1,5},{2,6},{3,7},{4,0},{5,1},{6,2},{7,3},{8,12},{9,13},{10,... | collective-permute-start | bytes 1572872 | tf_op jit(solution)/shard_map/ppermute | solution.py:29
  116.7 21.1 %collective-permute-start.19 = (bf16[64,2048]{1,0:T(8,128)(2,1)S(1)}, bf16[64,2048]{1,0:T(8,128)(2,1)S(1)}, u32[]{:S(2)}, u32[]{:S(2)}) collective-permute-start(bf16[64,2048]{1,0:T(8,128)(2,1)S(1)} %add_convert_fusion.5), channel_id=1, source_target_pairs={{0,16},{1,17},{2,18},{3,19},{4,20},{5,21},{6,22},{7,23},{8,24},{9,... | collective-permute-start | bytes 786440 | tf_op jit(solution)/shard_map/ppermute | solution.py:29
  120.0 11.7 %collective-permute-start.23 = (bf16[64,2048]{1,0:T(8,128)(2,1)S(1)}, bf16[64,2048]{1,0:T(8,128)(2,1)S(1)}, u32[]{:S(2)}, u32[]{:S(2)}) collective-permute-start(bf16[64,2048]{1,0:T(8,128)(2,1)S(1)} %add_convert_fusion.4), channel_id=1, source_target_pairs={{0,4},{1,5},{2,6},{3,7},{4,0},{5,1},{6,2},{7,3},{8,12},{9,13},{10,... | collective-permute-start | bytes 786440 | tf_op jit(solution)/shard_map/ppermute | solution.py:29
  129.0 6.4 %collective-permute-start.27 = (bf16[64,2048]{1,0:T(8,128)(2,1)S(1)}, bf16[64,2048]{1,0:T(8,128)(2,1)S(1)}, u32[]{:S(2)}, u32[]{:S(2)}) collective-permute-start(bf16[64,2048]{1,0:T(8,128)(2,1)S(1)} %add_convert_fusion.2), channel_id=1, source_target_pairs={{0,2},{1,3},{2,0},{3,1},{4,6},{5,7},{6,4},{7,5},{8,10},{9,11},{10,... | collective-permute-start | bytes 786440 | tf_op jit(solution)/shard_map/ppermute | solution.py:29
  131.8 8.4 %collective-permute-start.24 = (bf16[64,2048]{1,0:T(8,128)(2,1)S(1)}, bf16[64,2048]{1,0:T(8,128)(2,1)S(1)}, u32[]{:S(2)}, u32[]{:S(2)}) collective-permute-start(bf16[64,2048]{1,0:T(8,128)(2,1)S(1)} %add_convert_fusion.3), channel_id=1, source_target_pairs={{0,24},{1,25},{2,26},{3,27},{4,28},{5,29},{6,30},{7,31},{8,16},{9,... | collective-permute-start | bytes 786440 | tf_op jit(solution)/shard_map/ppermute | solution.py:29
  135.5 7.5 %collective-permute-start.28 = (bf16[64,2048]{1,0:T(8,128)(2,1)S(1)}, bf16[64,2048]{1,0:T(8,128)(2,1)S(1)}, u32[]{:S(2)}, u32[]{:S(2)}) collective-permute-start(bf16[64,2048]{1,0:T(8,128)(2,1)S(1)} %add_convert_fusion.1), channel_id=1, source_target_pairs={{0,8},{1,9},{2,10},{3,11},{4,12},{5,13},{6,14},{7,15},{8,0},{9,1},... | collective-permute-start | bytes 786440 | tf_op jit(solution)/shard_map/ppermute | solution.py:29
where the time goes:
time: 144 us
  waiting for transfers between devices  61.1 us (42%)
  starting transfers between devices  35.9 us (25%)
  Pallas kernels  27.4 us (19%)
  local copies, waits for them, and re-layouts  8.51 us (6%)
  blocking collectives  8.42 us (6%)
  other arithmetic  2.42 us (2%)
    ppermute x28, waiting for transfers between devices, swapped(): lax.ppermute(value, AXES, [(source, source ^ flip) for source in range(co...  60.4 us
    ppermute x28, starting transfers between devices, swapped(): lax.ppermute(value, AXES, [(source, source ^ flip) for source in range(co...  31 us
    pallas_call x5, Pallas kernels, run_expert(): pl.pallas_call(functools.partial(expert_kernel, len(pieces), n_outs, with...  26.1 us
    all_gather x1, blocking collectives, dense_plan(): grouped = lax.all_gather(group_mix, 'tp', axis=1, tiled=True)  8.42 us
    unnamed x24, local copies, waits for them, and re-layouts  7.64 us
    ppermute x1, starting transfers between devices, passed_along(): lax.ppermute(value, axis, [(source, source + steps) for source in range(i...  4.89 us
  transfers between devices with their start and end apart: 29, of which 15 were waited for; matrix products, arithmetic and copies ran while one was open for 2% of the time, Pallas kernels for 15%

commit v1 on v0

--- a/solution.py
+++ b/solution.py
@@ -132,7 +132,27 @@
     return (own_resid + routed + shared).astype(jnp.bfloat16)
 
 
-def pool_kernel(rim_ref, pooled_ref, weight_ref, scale_ref, out_ref):
+def brought(pairs, sems):
+    copies = [
+        pltpu.make_async_copy(source, target, sems.at[place])
+        for place, (source, target) in enumerate(pairs)
+    ]
+    for copy in copies:
+        copy.start()
+    return copies
+
+
+def pool_kernel(
+    rim_ref, pooled_hbm, weight_hbm, scale_hbm, *refs
+):
+    pieces, (mixed_ref, pooled_ref, weight_ref, scale_ref, sems) = refs[:-5], refs[-5:]
+    rows = pieces[0].shape[0] // 2
+    tp_index = lax.axis_index("tp")
+    copies = brought(
+        ((pooled_hbm, pooled_ref), (weight_hbm, weight_ref), (scale_hbm, scale_ref)), sems
+    )
+    for copy in copies:
+        copy.wait()
     tok_dev = pooled_ref.shape[0]
     window = lax.shift_left(jnp.int32(2), lax.axis_index("tp"))
     channels = pooled_ref[...].astype(jnp.float32)
@@ -146,39 +166,76 @@
     counted = jnp.minimum(position + 1, window).astype(jnp.float32)
     pooled = (chosen[REACH:] / counted - channels).astype(jnp.bfloat16)
     mixed = jnp.dot(pooled, weight_ref[0], preferred_element_type=jnp.float32)
-    out_ref[...] = (mixed * scale_ref[...]).astype(jnp.bfloat16)
-
-
-def norm_kernel(
-    grouped_ref, stream_ref, weight_ref, gain_ref, table_ref, packed_ref, resid_ref, wide_ref
-):
+    mixed_ref[...] = (mixed * scale_ref[...]).astype(jnp.bfloat16)
+    for flip, piece in enumerate(pieces):
+        for place, block in enumerate((tp_index ^ flip, tp_index ^ flip ^ X_BIT)):
+            begin = pl.multiple_of(block * rows, rows)
+            piece[place * rows : (place + 1) * rows] = mixed_ref[pl.ds(begin, rows)]
+
+
+def norm_kernel(*refs):
+    groups, refs = refs[:-15], refs[-15:]
+    routes_hbm, route_weights_hbm, stream_hbm, weight_hbm, gain_hbm = refs[:5]
+    packed_ref, resid_ref, wide_ref, stream_ref, weight_ref, gain_ref, table_ref = refs[5:12]
+    routes_ref, route_weights_ref, sems = refs[12:]
     rows, width = resid_ref.shape
+    parts, depth, _ = weight_ref.shape
     tp_index = lax.axis_index("tp")
-    own = pl.ds(pl.multiple_of(tp_index * rows, rows), rows)
-    peer = pl.ds(pl.multiple_of((tp_index ^ X_BIT) * rows, rows), rows)
-
-    def both(ref, cols=slice(None)):
-        return jnp.concatenate([ref[own, cols], ref[peer, cols]], 0)
-
-    grouped = both(grouped_ref)
+    places = [pl.multiple_of(block * rows, rows) for block in (tp_index, tp_index ^ X_BIT)]
+    pairs = []
+    for part in range(parts):
+        begin = pl.multiple_of((tp_index ^ part) * depth, depth)
+        pairs.append((weight_hbm.at[pl.ds(begin, depth)], weight_ref.at[part]))
+    for place, begin in enumerate(places):
+        pairs.append((stream_hbm.at[pl.ds(begin, rows)], stream_ref.at[pl.ds(place * rows, rows)]))
+    pairs.append((gain_hbm, gain_ref))
+    pairs = [(routes_hbm, routes_ref), (route_weights_hbm, route_weights_ref)] + pairs
+    first, second, *copies = brought(pairs, sems)
+    first.wait()
+    second.wait()
+
+    experts = lax.axis_size("sp")
+    named = routes_ref[...]
+    share = route_weights_ref[...]
+    shape = (table_ref.shape[1], named.shape[1])
+    line = lax.broadcasted_iota(jnp.int32, shape, 0)
+    table = jnp.zeros(shape, jnp.float32)
+    for choice in range(named.shape[0]):
+        asked = named[choice : choice + 1]
+        hit = (line == asked) | (line == asked + experts)
+        table = table + jnp.where(hit, share[choice : choice + 1], 0.0)
+    high = table.astype(jnp.bfloat16).astype(jnp.float32)
+    table = jnp.where(line < experts, high, table - high)
+    table_ref[...] = jnp.transpose(table).astype(jnp.bfloat16)
+    for place, begin in enumerate(places):
+        packed_ref[place * rows : (place + 1) * rows, width:] = table_ref[pl.ds(begin, rows)]
+
+    block = min(512, width)
+    blocks = [slice(start, start + block) for start in range(0, width, block)]
+    for part, group in enumerate(groups):
+        copies[part].wait()
+        for cols in blocks:
+            mixed = jnp.dot(
+                group[...], weight_ref[part, :, cols], preferred_element_type=jnp.float32
+            )
+            wide_ref[:, cols] = mixed if part == 0 else wide_ref[:, cols] + mixed
+    for copy in copies[parts:]:
+        copy.wait()
     squares = jnp.zeros((2 * rows, 1), jnp.float32)
-    block = min(512, width)
-    for start in range(0, width, block):
-        cols = slice(start, start + block)
-        mixed = jnp.dot(grouped, weight_ref[:, cols], preferred_element_type=jnp.float32)
-        residual = (both(stream_ref, cols).astype(jnp.float32) + mixed).astype(jnp.bfloat16)
+    for cols in blocks:
+        residual = (stream_ref[:, cols].astype(jnp.float32) + wide_ref[:, cols]).astype(
+            jnp.bfloat16
+        )
         resid_ref[:, cols] = residual[:rows]
         wide = residual.astype(jnp.float32)
         wide_ref[:, cols] = wide
         squares = squares + jnp.sum(wide * wide, axis=1, keepdims=True)
     factor = lax.rsqrt(squares / width + EPSILON)
-    for start in range(0, width, block):
-        cols = slice(start, start + block)
+    for cols in blocks:
         packed_ref[:, cols] = (wide_ref[:, cols] * factor * gain_ref[:, cols]).astype(jnp.bfloat16)
-    packed_ref[:, width:] = both(table_ref)
-
-
-def expert_kernel(n_pieces, n_outs, with_shared, *refs):
+
+
+def expert_kernel(n_pieces, takes, n_outs, with_shared, *refs):
     pieces = refs[:n_pieces]
     weights = refs[n_pieces : n_pieces + (12 if with_shared else 6)]
     outs = refs[n_pieces + len(weights) :][:n_outs]
@@ -187,10 +244,10 @@
     experts = lax.axis_size("sp")
     mine = lax.axis_index("sp")
     begin = 0
-    for piece in pieces:
-        count = piece.shape[0]
-        rows_ref[begin : begin + count] = piece[:, :width]
-        marks = piece[:, width:].astype(jnp.float32)
+    for place, first, count in takes:
+        taken = slice(first, first + count)
+        rows_ref[begin : begin + count] = pieces[place][taken, :width]
+        marks = pieces[place][taken, width:].astype(jnp.float32)
         lane = lax.broadcasted_iota(jnp.int32, marks.shape, 1)
         named = (lane == mine) | (lane == mine + experts)
         scale_ref[begin : begin + count] = jnp.sum(
@@ -235,18 +292,41 @@
             out[:, cols] = value[place * share : (place + 1) * share]
 
 
+def pass_kernel(source, target):
+    target[...] = source[...]
+
+
+def passing(token):
+    return pl.pallas_call(
+        pass_kernel,
+        out_shape=jax.ShapeDtypeStruct(token.shape, token.dtype),
+        in_specs=in_vmem(1),
+        out_specs=in_vmem(1)[0],
+        compiler_params=pltpu.CompilerParams(vmem_limit_bytes=MIB),
+    )(token)
+
+
 def in_vmem(count):
     return [pl.BlockSpec(memory_space=pltpu.VMEM)] * count
 
 
-def run_expert(pieces, weights, n_outs, width):
-    count = sum(piece.shape[0] for piece in pieces)
+def kept_in_hbm(*arrays):
+    return [pltpu.with_memory_space_constraint(array, pltpu.HBM) for array in arrays]
+
+
+def in_hbm(count):
+    return [pl.BlockSpec(memory_space=pltpu.HBM)] * count
+
+
+def run_expert(pieces, weights, n_outs, width, takes=None):
+    takes = takes or [(place, 0, piece.shape[0]) for place, piece in enumerate(pieces)]
+    count = sum(take[2] for take in takes)
     with_shared = len(weights) == 12
     hidden = weights[0].shape[1] * 2
     shared = weights[6].shape[1] * 2 if with_shared else 128
     out = jax.ShapeDtypeStruct((count // n_outs, width), jnp.bfloat16)
     return pl.pallas_call(
-        functools.partial(expert_kernel, len(pieces), n_outs, with_shared),
+        functools.partial(expert_kernel, len(pieces), tuple(takes), n_outs, with_shared),
         out_shape=[out] * n_outs,
         in_specs=in_vmem(len(pieces) + len(weights)),
         out_specs=in_vmem(n_outs),
@@ -284,80 +364,113 @@
     for weight in (shared_gate, shared_up, shared_down):
         shared_weights += [weight, swapped(weight, CORE_BIT)]
 
-    experts = jnp.arange(sp_size, dtype=jnp.int32)
-    table = jnp.sum(
-        jnp.where(routes[:, :, None] == experts, route_weights[:, :, None], 0.0), axis=1
-    )
-    high = lax.reduce_precision(table, 8, 7)
-    table = jnp.concatenate([high, table - high], 1).astype(bf16)
     lanes = -(-2 * sp_size // 128) * 128
-    table = jnp.pad(table, ((0, 0), (0, lanes - 2 * sp_size)))
-
-    group_mix = pl.pallas_call(
+    piece = jax.ShapeDtypeStruct((2 * rows, pooled_in.shape[1]), bf16)
+    pool = pl.pallas_call(
         pool_kernel,
-        out_shape=jax.ShapeDtypeStruct(pooled_in.shape, bf16),
-        in_specs=in_vmem(4),
-        out_specs=in_vmem(1)[0],
+        out_shape=[piece] * tp_size,
+        in_specs=in_vmem(1) + in_hbm(3),
+        out_specs=in_vmem(tp_size),
+        scratch_shapes=[
+            pltpu.VMEM(pooled_in.shape, bf16),
+            pltpu.VMEM(pooled_in.shape, bf16),
+            pltpu.VMEM(pool_weight.shape, bf16),
+            pltpu.VMEM((1, pool_scale.size), f32),
+            pltpu.SemaphoreType.DMA((3,)),
+        ],
         compiler_params=pltpu.CompilerParams(vmem_limit_bytes=4 * MIB),
-    )(rim_rows, pooled_in, pool_weight, pool_scale[None])
-    grouped = lax.all_gather(group_mix, "tp", axis=1, tiled=True)
+    )
+    rim_rows, weights[1], weights[3] = tied(rim_rows, weights[1], weights[3])
+    groups = pool(rim_rows, *kept_in_hbm(pooled_in, pool_weight, pool_scale[None]))
+    groups = [swapped(group, flip) if flip else group for flip, group in enumerate(groups)]
+    depth = out_weight.shape[0] // tp_size
     pair, own_resid = pl.pallas_call(
         norm_kernel,
         out_shape=[
             jax.ShapeDtypeStruct((2 * rows, width + lanes), bf16),
             jax.ShapeDtypeStruct((rows, width), bf16),
         ],
-        in_specs=in_vmem(5),
+        in_specs=in_vmem(tp_size) + in_hbm(5),
         out_specs=in_vmem(2),
-        scratch_shapes=[pltpu.VMEM((2 * rows, width), f32)],
+        scratch_shapes=[
+            pltpu.VMEM((2 * rows, width), f32),
+            pltpu.VMEM((2 * rows, width), bf16),
+            pltpu.VMEM((tp_size, depth, width), bf16),
+            pltpu.VMEM((1, width), f32),
+            pltpu.VMEM((tok_dev, lanes), bf16),
+            pltpu.VMEM(routes.shape[::-1], jnp.int32),
+            pltpu.VMEM(routes.shape[::-1], f32),
+            pltpu.SemaphoreType.DMA((tp_size + 5,)),
+        ],
         compiler_params=pltpu.CompilerParams(vmem_limit_bytes=10 * MIB),
-    )(grouped, stream, out_weight, norm_gain[None], table)
+    )(
+        *groups,
+        *kept_in_hbm(routes.T, route_weights.T, stream, out_weight, norm_gain[None]),
+    )
 
     kept, sent, got = {}, {}, {}
     z_1, z_2, _ = z_bits[1:]
     far_2 = swapped(pair[:rows], z_2)
     near = swapped(pair, y_bit)
-    next_z = swapped(pair, z_1)
     (kept[0],) = run_expert([pair], weights + shared_weights, 1, width)
     far_2, kept[0] = tied(far_2, kept[0])
     far_3 = swapped(far_2, z_1)
     y_2 = swapped(far_2, y_bit)
     x_2 = swapped(far_2, X_BIT)
     near, far_2 = tied(near, far_2)
+    pair, far_2 = tied(pair, far_2)
+    next_z = swapped(pair, z_1)
+    other_z = swapped(near, z_1)
     (sent[0],) = run_expert([near], weights, 1, width)
-    far_3, sent[0] = tied(far_3, sent[0])
+    y_2, sent[0] = tied(y_2, sent[0])
+    xy_2 = swapped(y_2, X_BIT)
+    far_3, y_2 = tied(far_3, y_2)
     y_3 = swapped(far_3, y_bit)
     x_3 = swapped(far_3, X_BIT)
-    y_2, far_3 = tied(y_2, far_3)
-    xy_2 = swapped(y_2, X_BIT)
-    next_z, y_2 = tied(next_z, y_2)
-    y_1 = swapped(next_z, y_bit)
-    sent[0], next_z = tied(sent[0], next_z)
+    token = passing(jnp.zeros((8, 128), f32))
+    y_3, far_3 = tied(y_3, far_3)
+    xy_3 = swapped(y_3, X_BIT)
+    sent[0], y_3 = tied(sent[0], y_3)
     got[0] = swapped(sent[0], y_bit)
-    y_3, next_z = tied(y_3, next_z)
-    xy_3 = swapped(y_3, X_BIT)
     xy_2, y_3 = tied(xy_2, y_3)
-    kept[2], sent[2] = run_expert([far_2, y_2, x_2, xy_2], weights, 2, width)
+    blocks = [(place, 0, rows) for place in range(4)]
+    kept[2], sent[2] = run_expert([far_2, y_2, x_2, xy_2, token], weights, 2, width, blocks)
     got[2] = swapped(sent[2], X_BIT)
+    token = passing(token)
     xy_3, sent[2] = tied(xy_3, sent[2])
-    kept[3], sent[3] = run_expert([far_3, y_3, x_3, xy_3], weights, 2, width)
-    got[3] = swapped(sent[3], X_BIT)
-    y_1, sent[3] = tied(y_1, sent[3])
-    kept[1], sent[1] = run_expert([next_z, y_1], weights, 2, width)
-    got[1] = swapped(sent[1], y_bit)
+    kept[3], sent[3] = run_expert([far_3, x_3, y_3, xy_3, token], weights, 2, width, blocks)
+    got[3] = swapped(sent[3], y_bit)
+    next_z, sent[3] = tied(next_z, sent[3])
+    takes = [(0, 0, rows), (1, 0, rows), (0, rows, rows), (1, rows, rows)]
+    kept[1], sent[1] = run_expert([next_z, other_z], weights, 2, width, takes)
+    got[1] = swapped(sent[1], X_BIT)
 
     def half(k, which):
         part = slice(which * rows, (which + 1) * rows)
         return kept[k][part].astype(f32) + got[k][part].astype(f32)
 
+    def passed_on(k):
+        flip = y_bit if k in (1, 2) else X_BIT
+        return swapped(half(k, 1).astype(bf16), flip)
+
+    def finished(k):
+        flow = (half(k, 0) + more[k].astype(f32)).astype(bf16)
+        return swapped(flow, z_bits[k])
+
     more, flows = {}, {}
-    for k in (2, 0, 3, 1):
-        flip = X_BIT if k < 2 else y_bit
-        more[k] = swapped(half(k, 1).astype(bf16), flip)
-    for k in (2, 3, 1):
-        flow = (half(k, 0) + more[k].astype(f32)).astype(bf16)
-        flows[k] = swapped(flow, z_bits[k])
-    result = half(0, 0) + more[0].astype(f32) + own_resid.astype(f32)
+    got[2], sent[1] = tied(got[2], sent[1])
+    more[2] = passed_on(2)
+    more[0] = passed_on(0)
+    got[3], got[2] = tied(got[3], got[2])
+    more[3] = passed_on(3)
+    more[2], got[3] = tied(more[2], got[3])
+    flows[2] = finished(2)
+    wide = passing(own_resid.astype(f32))
+    base = passing(half(0, 0) + wide)
+    more[1] = passed_on(1)
+    flows[3] = finished(3)
+    flows[1] = finished(1)
+    result = base + more[0].astype(f32)
     for k in (2, 3, 1):
         result = result + flows[k].astype(f32)
     return result.astype(bf16)

time: 144 us -> 141 us (0.979)
  waiting for transfers between devices: 61.1 us -> 78.5 us
  blocking collectives: 8.42 us -> 0 us
  Pallas kernels: 27.4 us -> 20 us
  local copies, waits for them, and re-layouts: 8.51 us -> 3.85 us
    ppermute x28 -> x31, waiting for transfers between devices: 60.4 us -> 77.2 us  [swapped(): lax.ppermute(value, AXES, [(source, source ^ flip) for source in range(co...]
    pallas_call x6 -> x10, Pallas kernels: 26.5 us -> 16.9 us  [the longest x5 15.3 us: run_expert(): pl.pallas_call(functools.partial(expert_kernel, len(pieces), tuple(takes)...]
    all_gather x1 -> x0, blocking collectives: 8.42 us -> none  [dense_plan(): grouped = lax.all_gather(group_mix, 'tp', axis=1, tiled=True)]
    unnamed x24 -> x12, local copies, waits for them, and re-layouts: 7.64 us -> 3.13 us
    pallas_call x1, Pallas kernels: 0.95 us -> 3.1 us  [dense_plan(): pl.pallas_call(norm_kernel, out_shape=[jax.ShapeDtypeStruct((2 * rows, wi...]
    ppermute x28 -> x31, starting transfers between devices: 31 us -> 32.1 us  [swapped(): lax.ppermute(value, AXES, [(source, source ^ flip) for source in range(co...]
  transfers between devices with their start and end apart: 29 -> 32, of which waited for: 15 -> 18; matrix products, arithmetic and copies ran while one was open for 2% -> 1% of each run, Pallas kernels for 15% -> 14%
where the time goes in v1:
time: 141 us
  waiting for transfers between devices  78.5 us (56%)
  starting transfers between devices  37 us (26%)
  Pallas kernels  20 us (14%)
  local copies, waits for them, and re-layouts  3.85 us (3%)
  other arithmetic  1.55 us (1%)
    ppermute x31, waiting for transfers between devices, swapped(): lax.ppermute(value, AXES, [(source, source ^ flip) for source in range(co...  77.2 us
    ppermute x31, starting transfers between devices, swapped(): lax.ppermute(value, AXES, [(source, source ^ flip) for source in range(co...  32.1 us
    pallas_call x5, Pallas kernels, run_expert(): pl.pallas_call(functools.partial(expert_kernel, len(pieces), tuple(takes)...  15.3 us
    ppermute x1, starting transfers between devices, passed_along(): lax.ppermute(value, axis, [(source, source + steps) for source in range(i...  4.89 us
    unnamed x12, local copies, waits for them, and re-layouts  3.13 us
    pallas_call x1, Pallas kernels, dense_plan(): pl.pallas_call(norm_kernel, out_shape=[jax.ShapeDtypeStruct((2 * rows, wi...  3.1 us
  transfers between devices with their start and end apart: 32, of which 18 were waited for; matrix products, arithmetic and copies ran while one was open for 1% of the time, Pallas kernels for 14%

profile of v1, /device:TPU:0, one launch (start us, length us, event | category | flops | bytes accessed | tf_op | source)
XLA Modules:
  0.0 141.1 jit_solution(5701869086194076033)
XLA Ops:
  0.0 0.5 collective-permute-start.1
  0.5 0.5 collective-permute-start.7
  1.0 0.7 slice.54
  1.7 4.9 %collective-permute-start = (bf16[16,256]{1,0:T(8,128)(2,1)S(1)}, bf16[16,256]{1,0:T(8,128)(2,1)S(1)}, u32[]{:S(2)}, u32[]{:S(2)}) collective-permute-start(bf16[16,256]{1,0:T(8,128)(2,1)S(1)} %slice.54), channel_id=1, source_target_pairs={{0,4},{4,8},{8,12},{12,16},{16,20},{20,24},{24,28},{1,5},{5,9},{9,... | collective-permute-start | bytes 24584 | tf_op jit(solution)/shard_map/ppermute | solution.py:24
  6.6 1.3 collective-permute-done.rim_ref
  8.0 0.5 collective-permute-start.9
  8.5 1.5 %shard_map.136 = (bf16[128,256]{1,0:T(8,128)(2,1)S(1)}, bf16[128,256]{1,0:T(8,128)(2,1)S(1)}, bf16[128,256]{1,0:T(8,128)(2,1)S(1)}, bf16[128,256]{1,0:T(8,128)(2,1)S(1)}) custom-call(bf16[16,256]{1,0:T(8,128)(2,1)S(1)} %collective-permute-done.rim_ref, bf16[256,256]{1,0:T(8,128)(2,1)} %pooled_hbm.1, bf16[1,256,256]{2,1,0:T(8,128)(2,1)} %weight_hbm.1, ...), custom_call_target="tpu_custom_call" | custom-call | tf_op jit(solution)/shard_map/pallas_call | solution.py:384
  10.0 0.1 collective-permute-start.3
  10.1 2.8 %collective-permute-done.3.refs_1_ = bf16[128,256]{1,0:T(8,128)(2,1)S(1)} collective-permute-done((bf16[128,256]{1,0:T(8,128)(2,1)S(1)}, bf16[128,256]{1,0:T(8,128)(2,1)S(1)}, u32[]{:S(2)}, u32[]{:S(2)}) %collective-permute-start.3) | collective-permute-done | bytes 65568 | tf_op jit(solution)/shard_map/ppermute | solution.py:29
  12.8 2.8 %collective-permute-start.4 = (bf16[128,256]{1,0:T(8,128)(2,1)S(1)}, bf16[128,256]{1,0:T(8,128)(2,1)S(1)}, u32[]{:S(2)}, u32[]{:S(2)}) collective-permute-start(bf16[128,256]{1,0:T(8,128)(2,1)S(1)} %get-tuple-element.46), channel_id=1, source_target_pairs={{0,2},{1,3},{2,0},{3,1},{4,6},{5,7},{6,4},{7,5},{8,10},{9,11},{10,... | collective-permute-start | bytes 196616 | tf_op jit(solution)/shard_map/ppermute | solution.py:29
  15.7 2.4 %collective-permute-done.4.refs_2_ = bf16[128,256]{1,0:T(8,128)(2,1)S(1)} collective-permute-done((bf16[128,256]{1,0:T(8,128)(2,1)S(1)}, bf16[128,256]{1,0:T(8,128)(2,1)S(1)}, u32[]{:S(2)}, u32[]{:S(2)}) %collective-permute-start.4) | collective-permute-done | bytes 65568 | tf_op jit(solution)/shard_map/ppermute | solution.py:29
  18.1 0.5 collective-permute-start.5
  18.5 3.5 %collective-permute-done.5.refs_3_ = bf16[128,256]{1,0:T(8,128)(2,1)S(1)} collective-permute-done((bf16[128,256]{1,0:T(8,128)(2,1)S(1)}, bf16[128,256]{1,0:T(8,128)(2,1)S(1)}, u32[]{:S(2)}, u32[]{:S(2)}) %collective-permute-start.5) | collective-permute-done | bytes 65568 | tf_op jit(solution)/shard_map/ppermute | solution.py:29
  22.0 3.1 %shard_map.137 = (bf16[128,2176]{1,0:T(8,128)(2,1)S(1)}, bf16[64,2048]{1,0:T(8,128)(2,1)S(1)}) custom-call(bf16[128,256]{1,0:T(8,128)(2,1)S(1)} %get-tuple-element.44.refs_0_, bf16[128,256]{1,0:T(8,128)(2,1)S(1)} %collective-permute-done.3.refs_1_, bf16[128,256]{1,0:T(8,128)(2,1)S(1)} %collective-permute-done.4.refs_2_, ...), custom_call_target="tpu_custom_call" | custom-call | tf_op jit(solution)/shard_map/pallas_call | solution.py:387
  25.2 2.4 %collective-permute-start.12 = (bf16[128,2176]{1,0:T(8,128)(2,1)S(1)}, bf16[128,2176]{1,0:T(8,128)(2,1)S(1)}, u32[]{:S(2)}, u32[]{:S(2)}) collective-permute-start(bf16[128,2176]{1,0:T(8,128)(2,1)S(1)} %get-tuple-element.71.refs_0_), channel_id=1, source_target_pairs={{0,4},{1,5},{2,6},{3,7},{4,0},{5,1},{6,2},{7,3},{8,12},{9,13},{10,... | collective-permute-start | bytes 1671176 | tf_op jit(solution)/shard_map/ppermute | solution.py:29
  27.5 2.6 %collective-permute-start.6 = (bf16[64,2176]{1,0:T(8,128)(2,1)S(1)}, bf16[64,2176]{1,0:T(8,128)(2,1)S(1)}, u32[]{:S(2)}, u32[]{:S(2)}) collective-permute-start(bf16[64,2176]{1,0:T(8,128)(2,1)S(1)} %slice.55), channel_id=1, source_target_pairs={{0,16},{1,17},{2,18},{3,19},{4,20},{5,21},{6,22},{7,23},{8,24},{9,... | collective-permute-start | bytes 835592 | tf_op jit(solution)/shard_map/ppermute | solution.py:29
  30.2 1.0 copy-done.3
  31.2 1.0 copy-done.4
  32.3 1.0 copy-done.5
  33.3 2.6 %shard_map.138 = bf16[128,2048]{1,0:T(8,128)(2,1)S(1)} custom-call(bf16[128,2176]{1,0:T(8,128)(2,1)S(1)} %get-tuple-element.71.refs_0_, bf16[2048,512]{1,0:T(8,128)(2,1)S(1)} %bitcast.8, bf16[2048,512]{1,0:T(8,128)(2,1)S(1)} %collective-permute-done.1.refs_2_.refs_6_.refs_3_, bf16[2048,512]{1,0:T(8,128)(2,1)S(1)} %bitcast.14, ...), custom_call_target="tpu_custom_call" | custom-call | tf_op jit(solution)/shard_map/pallas_call | solution.py:328
  35.9 6.9 %collective-permute-done.6.refs_0_ = bf16[64,2176]{1,0:T(8,128)(2,1)S(1)} collective-permute-done((bf16[64,2176]{1,0:T(8,128)(2,1)S(1)}, bf16[64,2176]{1,0:T(8,128)(2,1)S(1)}, u32[]{:S(2)}, u32[]{:S(2)}) %collective-permute-start.6) | collective-permute-done | bytes 278560 | tf_op jit(solution)/shard_map/ppermute | solution.py:29
  42.8 0.5 collective-permute-start.11
  43.3 0.7 collective-permute-start.13
  44.0 1.9 %shard_map.139 = bf16[128,2048]{1,0:T(8,128)(2,1)S(1)} custom-call(bf16[128,2176]{1,0:T(8,128)(2,1)S(1)} %collective-permute-done.12.refs_0_, bf16[2048,512]{1,0:T(8,128)(2,1)S(1)} %bitcast.9, bf16[2048,512]{1,0:T(8,128)(2,1)S(1)} %collective-permute-done.1.refs_2_.refs_6_.refs_3_, bf16[2048,512]{1,0:T(8,128)(2,1)S(1)} %bitcast.15, ...), custom_call_target="tpu_custom_call" | custom-call | tf_op jit(solution)/shard_map/pallas_call | solution.py:328
  45.9 4.5 %collective-permute-done.11.refs_1_ = bf16[64,2176]{1,0:T(8,128)(2,1)S(1)} collective-permute-done((bf16[64,2176]{1,0:T(8,128)(2,1)S(1)}, bf16[64,2176]{1,0:T(8,128)(2,1)S(1)}, u32[]{:S(2)}, u32[]{:S(2)}) %collective-permute-start.11) | collective-permute-done | bytes 278560 | tf_op jit(solution)/shard_map/ppermute | solution.py:29
  50.4 0.4 collective-permute-done.13.refs_0_
  50.8 1.3 collective-permute-start.14
  52.1 2.0 %collective-permute-start.17 = (bf16[64,2176]{1,0:T(8,128)(2,1)S(1)}, bf16[64,2176]{1,0:T(8,128)(2,1)S(1)}, u32[]{:S(2)}, u32[]{:S(2)}) collective-permute-start(bf16[64,2176]{1,0:T(8,128)(2,1)S(1)} %collective-permute-done.6.refs_0_), channel_id=1, source_target_pairs={{0,2},{1,3},{2,0},{3,1},{4,6},{5,7},{6,4},{7,5},{8,10},{9,11},{10,... | collective-permute-start | bytes 835592 | tf_op jit(solution)/shard_map/ppermute | solution.py:29
  54.1 1.7 %collective-permute-start.23 = (bf16[128,2176]{1,0:T(8,128)(2,1)S(1)}, bf16[128,2176]{1,0:T(8,128)(2,1)S(1)}, u32[]{:S(2)}, u32[]{:S(2)}) collective-permute-start(bf16[128,2176]{1,0:T(8,128)(2,1)S(1)} %get-tuple-element.71.refs_0_), channel_id=1, source_target_pairs={{0,8},{1,9},{2,10},{3,11},{4,12},{5,13},{6,14},{7,15},{8,0},{9,1},... | collective-permute-start | bytes 1671176 | tf_op jit(solution)/shard_map/ppermute | solution.py:29
  55.8 0.3 collective-permute-start.24
  56.2 1.3 collective-permute-done.14.refs_2_
  57.5 4.0 %collective-permute-done.18.refs_3_ = bf16[64,2176]{1,0:T(8,128)(2,1)S(1)} collective-permute-done((bf16[64,2176]{1,0:T(8,128)(2,1)S(1)}, bf16[64,2176]{1,0:T(8,128)(2,1)S(1)}, u32[]{:S(2)}, u32[]{:S(2)}) %collective-permute-start.18) | collective-permute-done | bytes 278560 | tf_op jit(solution)/shard_map/ppermute | solution.py:29
  61.5 3.0 %collective-permute-done.17.refs_2_ = bf16[64,2176]{1,0:T(8,128)(2,1)S(1)} collective-permute-done((bf16[64,2176]{1,0:T(8,128)(2,1)S(1)}, bf16[64,2176]{1,0:T(8,128)(2,1)S(1)}, u32[]{:S(2)}, u32[]{:S(2)}) %collective-permute-start.17) | collective-permute-done | bytes 278560 | tf_op jit(solution)/shard_map/ppermute | solution.py:29
  64.4 3.5 %shard_map.143 = (bf16[128,2048]{1,0:T(8,128)(2,1)S(1)}, bf16[128,2048]{1,0:T(8,128)(2,1)S(1)}) custom-call(bf16[64,2176]{1,0:T(8,128)(2,1)S(1)} %collective-permute-done.6.refs_0_, bf16[64,2176]{1,0:T(8,128)(2,1)S(1)} %collective-permute-done.11.refs_1_, bf16[64,2176]{1,0:T(8,128)(2,1)S(1)} %collective-permute-done.17.refs_2_, ...), custom_call_target="tpu_custom_call" | custom-call | tf_op jit(solution)/shard_map/pallas_call | solution.py:328
  68.0 0.3 collective-permute-start.22
  68.3 1.7 %collective-permute-start.20 = (bf16[64,2176]{1,0:T(8,128)(2,1)S(1)}, bf16[64,2176]{1,0:T(8,128)(2,1)S(1)}, u32[]{:S(2)}, u32[]{:S(2)}) collective-permute-start(bf16[64,2176]{1,0:T(8,128)(2,1)S(1)} %collective-permute-done.14.refs_2_), channel_id=1, source_target_pairs={{0,2},{1,3},{2,0},{3,1},{4,6},{5,7},{6,4},{7,5},{8,10},{9,11},{10,... | collective-permute-start | bytes 835592 | tf_op jit(solution)/shard_map/ppermute | solution.py:29
  70.1 0.3 collective-permute-start.19
  70.3 17.4 %collective-permute-done.20.refs_3_ = bf16[64,2176]{1,0:T(8,128)(2,1)S(1)} collective-permute-done((bf16[64,2176]{1,0:T(8,128)(2,1)S(1)}, bf16[64,2176]{1,0:T(8,128)(2,1)S(1)}, u32[]{:S(2)}, u32[]{:S(2)}) %collective-permute-start.20) | collective-permute-done | bytes 278560 | tf_op jit(solution)/shard_map/ppermute | solution.py:29
  87.8 0.8 collective-permute-start.15
  88.6 2.1 %collective-permute-done.19.refs_1_ = bf16[64,2176]{1,0:T(8,128)(2,1)S(1)} collective-permute-done((bf16[64,2176]{1,0:T(8,128)(2,1)S(1)}, bf16[64,2176]{1,0:T(8,128)(2,1)S(1)}, u32[]{:S(2)}, u32[]{:S(2)}) %collective-permute-start.19) | collective-permute-done | bytes 278560 | tf_op jit(solution)/shard_map/ppermute | solution.py:29
  90.7 3.7 %shard_map.145 = (bf16[128,2048]{1,0:T(8,128)(2,1)S(1)}, bf16[128,2048]{1,0:T(8,128)(2,1)S(1)}) custom-call(bf16[64,2176]{1,0:T(8,128)(2,1)S(1)} %collective-permute-done.13.refs_0_, bf16[64,2176]{1,0:T(8,128)(2,1)S(1)} %collective-permute-done.19.refs_1_, bf16[64,2176]{1,0:T(8,128)(2,1)S(1)} %collective-permute-done.14.refs_2_, ...), custom_call_target="tpu_custom_call" | custom-call | tf_op jit(solution)/shard_map/pallas_call | solution.py:328
  94.5 0.8 collective-permute-start.21
  95.3 3.5 %shard_map.146 = (bf16[128,2048]{1,0:T(8,128)(2,1)S(1)}, bf16[128,2048]{1,0:T(8,128)(2,1)S(1)}) custom-call(bf16[128,2176]{1,0:T(8,128)(2,1)S(1)} %collective-permute-done.23.refs_0_, bf16[128,2176]{1,0:T(8,128)(2,1)S(1)} %collective-permute-done.24.refs_1_, bf16[2048,512]{1,0:T(8,128)(2,1)S(1)} %bitcast.12, ...), custom_call_target="tpu_custom_call" | custom-call | tf_op jit(solution)/shard_map/pallas_call | solution.py:328
  98.9 0.6 collective-permute-start.29
  99.5 0.1 add_convert_fusion.6
  99.6 1.3 collective-permute-start.25
  100.9 0.2 add_convert_fusion.7
  101.0 1.5 %collective-permute-start.16 = (bf16[64,2048]{1,0:T(8,128)(2,1)S(1)}, bf16[64,2048]{1,0:T(8,128)(2,1)S(1)}, u32[]{:S(2)}, u32[]{:S(2)}) collective-permute-start(bf16[64,2048]{1,0:T(8,128)(2,1)S(1)} %get-tuple-element.81), channel_id=1, source_target_pairs={{0,2},{1,3},{2,0},{3,1},{4,6},{5,7},{6,4},{7,5},{8,10},{9,11},{10,... | collective-permute-start | bytes 786440 | tf_op jit(solution)/shard_map/ppermute | solution.py:29
  102.6 8.4 %collective-permute-done.21 = bf16[128,2048]{1,0:T(8,128)(2,1)S(1)} collective-permute-done((bf16[128,2048]{1,0:T(8,128)(2,1)S(1)}, bf16[128,2048]{1,0:T(8,128)(2,1)S(1)}, u32[]{:S(2)}, u32[]{:S(2)}) %collective-permute-start.21) | collective-permute-done | bytes 524320 | tf_op jit(solution)/shard_map/ppermute | solution.py:29
  111.0 2.8 %collective-permute-done.25 = bf16[64,2048]{1,0:T(8,128)(2,1)S(1)} collective-permute-done((bf16[64,2048]{1,0:T(8,128)(2,1)S(1)}, bf16[64,2048]{1,0:T(8,128)(2,1)S(1)}, u32[]{:S(2)}, u32[]{:S(2)}) %collective-permute-start.25) | collective-permute-done | bytes 262176 | tf_op jit(solution)/shard_map/ppermute | solution.py:29
  113.8 0.1 add_convert_fusion.5
  113.9 5.5 %collective-permute-start.26 = (bf16[64,2048]{1,0:T(8,128)(2,1)S(1)}, bf16[64,2048]{1,0:T(8,128)(2,1)S(1)}, u32[]{:S(2)}, u32[]{:S(2)}) collective-permute-start(bf16[64,2048]{1,0:T(8,128)(2,1)S(1)} %add_convert_fusion.5), channel_id=1, source_target_pairs={{0,16},{1,17},{2,18},{3,19},{4,20},{5,21},{6,22},{7,23},{8,24},{9,... | collective-permute-start | bytes 786440 | tf_op jit(solution)/shard_map/ppermute | solution.py:29
  119.5 0.4 collective-permute-start.27
  119.8 0.1 add_convert_fusion.2
  119.9 0.6 collective-permute-start.30
  120.5 5.4 %collective-permute-done.27 = bf16[64,2048]{1,0:T(8,128)(2,1)S(1)} collective-permute-done((bf16[64,2048]{1,0:T(8,128)(2,1)S(1)}, bf16[64,2048]{1,0:T(8,128)(2,1)S(1)}, u32[]{:S(2)}, u32[]{:S(2)}) %collective-permute-start.27) | collective-permute-done | bytes 262176 | tf_op jit(solution)/shard_map/ppermute | solution.py:29
  125.9 0.1 add_convert_fusion.3
  126.0 0.8 collective-permute-start.28
  126.8 0.1 add_convert_fusion.1
  126.9 1.1 collective-permute-start.31
  128.0 5.2 %collective-permute-done.26 = bf16[64,2048]{1,0:T(8,128)(2,1)S(1)} collective-permute-done((bf16[64,2048]{1,0:T(8,128)(2,1)S(1)}, bf16[64,2048]{1,0:T(8,128)(2,1)S(1)}, u32[]{:S(2)}, u32[]{:S(2)}) %collective-permute-start.26) | collective-permute-done | bytes 262176 | tf_op jit(solution)/shard_map/ppermute | solution.py:29
  133.2 2.3 %collective-permute-done.28 = bf16[64,2048]{1,0:T(8,128)(2,1)S(1)} collective-permute-done((bf16[64,2048]{1,0:T(8,128)(2,1)S(1)}, bf16[64,2048]{1,0:T(8,128)(2,1)S(1)}, u32[]{:S(2)}, u32[]{:S(2)}) %collective-permute-start.28) | collective-permute-done | bytes 262176 | tf_op jit(solution)/shard_map/ppermute | solution.py:29
  135.5 4.8 %collective-permute-done.31 = bf16[64,2048]{1,0:T(8,128)(2,1)S(1)} collective-permute-done((bf16[64,2048]{1,0:T(8,128)(2,1)S(1)}, bf16[64,2048]{1,0:T(8,128)(2,1)S(1)}, u32[]{:S(2)}, u32[]{:S(2)}) %collective-permute-start.31) | collective-permute-done | bytes 262176 | tf_op jit(solution)/shard_map/ppermute | solution.py:29
  140.3 0.9 add_convert_fusion
  (35 shorter events, 0.3 us)
Async XLA Ops:
  0.0 8.0 %collective-permute-start.1 = (bf16[2048,512]{1,0:T(8,128)(2,1)}, bf16[2048,512]{1,0:T(8,128)(2,1)S(1)}, u32[]{:S(2)}, u32[]{:S(2)}) collective-permute-start(bf16[2048,512]{1,0:T(8,128)(2,1)} %bitcast.7), channel_id=1, source_target_pairs={{0,1},{1,0},{2,3},{3,2},{4,5},{5,4},{6,7},{7,6},{8,9},{9,8},{10,11... | collective-permute-start | bytes 6291464 | tf_op jit(solution)/shard_map/ppermute | solution.py:29
  0.5 8.0 %collective-permute-start.2 = (bf16[2048,512]{1,0:T(8,128)(2,1)}, bf16[2048,512]{1,0:T(8,128)(2,1)S(1)}, u32[]{:S(2)}, u32[]{:S(2)}) collective-permute-start(bf16[2048,512]{1,0:T(8,128)(2,1)} %bitcast.13), channel_id=1, source_target_pairs={{0,1},{1,0},{2,3},{3,2},{4,5},{5,4},{6,7},{7,6},{8,9},{9,8},{10,11... | collective-permute-start | bytes 6291464 | tf_op jit(solution)/shard_map/ppermute | solution.py:29
  0.5 29.6 %collective-permute-start.7 = (bf16[512,2048]{1,0:T(8,128)(2,1)}, bf16[512,2048]{1,0:T(8,128)(2,1)S(1)}, u32[]{:S(2)}, u32[]{:S(2)}) collective-permute-start(bf16[512,2048]{1,0:T(8,128)(2,1)} %bitcast.19), channel_id=1, source_target_pairs={{0,1},{1,0},{2,3},{3,2},{4,5},{5,4},{6,7},{7,6},{8,9},{9,8},{10,11... | collective-permute-start | bytes 6291464 | tf_op jit(solution)/shard_map/ppermute | solution.py:29
  1.0 26.5 %collective-permute-start.10 = (bf16[128,2048]{1,0:T(8,128)(2,1)}, bf16[128,2048]{1,0:T(8,128)(2,1)S(1)}, u32[]{:S(2)}, u32[]{:S(2)}) collective-permute-start(bf16[128,2048]{1,0:T(8,128)(2,1)} %refs_11_.1), channel_id=1, source_target_pairs={{0,1},{1,0},{2,3},{3,2},{4,5},{5,4},{6,7},{7,6},{8,9},{9,8},{10,11... | collective-permute-start | bytes 1572872 | tf_op jit(solution)/shard_map/ppermute | solution.py:29
  1.7 6.2 %collective-permute-start = (bf16[16,256]{1,0:T(8,128)(2,1)S(1)}, bf16[16,256]{1,0:T(8,128)(2,1)S(1)}, u32[]{:S(2)}, u32[]{:S(2)}) collective-permute-start(bf16[16,256]{1,0:T(8,128)(2,1)S(1)} %slice.54), channel_id=1, source_target_pairs={{0,4},{4,8},{8,12},{12,16},{16,20},{20,24},{24,28},{1,5},{5,9},{9,... | collective-permute-start | bytes 24584 | tf_op jit(solution)/shard_map/ppermute | solution.py:24
  8.0 22.2 %collective-permute-start.8 = (bf16[2048,128]{1,0:T(8,128)(2,1)}, bf16[2048,128]{1,0:T(8,128)(2,1)S(1)}, u32[]{:S(2)}, u32[]{:S(2)}) collective-permute-start(bf16[2048,128]{1,0:T(8,128)(2,1)} %refs_7_.3), channel_id=1, source_target_pairs={{0,1},{1,0},{2,3},{3,2},{4,5},{5,4},{6,7},{7,6},{8,9},{9,8},{10,11... | collective-permute-start | bytes 1572872 | tf_op jit(solution)/shard_map/ppermute | solution.py:29
  8.0 22.2 %collective-permute-start.9 = (bf16[2048,128]{1,0:T(8,128)(2,1)}, bf16[2048,128]{1,0:T(8,128)(2,1)S(1)}, u32[]{:S(2)}, u32[]{:S(2)}) collective-permute-start(bf16[2048,128]{1,0:T(8,128)(2,1)} %refs_9_.1), channel_id=1, source_target_pairs={{0,1},{1,0},{2,3},{3,2},{4,5},{5,4},{6,7},{7,6},{8,9},{9,8},{10,11... | collective-permute-start | bytes 1572872 | tf_op jit(solution)/shard_map/ppermute | solution.py:29
  8.5 21.7 %copy-start.2 = (bf16[1,512,2048]{2,1,0:T(8,128)(2,1)S(1)}, bf16[1,512,2048]{2,1,0:T(8,128)(2,1)}, u32[]{:S(2)}) copy-start(bf16[1,512,2048]{2,1,0:T(8,128)(2,1)} %param.24) | copy-start | bytes 6291460
  10.0 2.9 %collective-permute-start.3 = (bf16[128,256]{1,0:T(8,128)(2,1)S(1)}, bf16[128,256]{1,0:T(8,128)(2,1)S(1)}, u32[]{:S(2)}, u32[]{:S(2)}) collective-permute-start(bf16[128,256]{1,0:T(8,128)(2,1)S(1)} %get-tuple-element.45), channel_id=1, source_target_pairs={{0,1},{1,0},{2,3},{3,2},{4,5},{5,4},{6,7},{7,6},{8,9},{9,8},{10,11... | collective-permute-start | bytes 196616 | tf_op jit(solution)/shard_map/ppermute | solution.py:29
  12.8 5.2 %collective-permute-start.4 = (bf16[128,256]{1,0:T(8,128)(2,1)S(1)}, bf16[128,256]{1,0:T(8,128)(2,1)S(1)}, u32[]{:S(2)}, u32[]{:S(2)}) collective-permute-start(bf16[128,256]{1,0:T(8,128)(2,1)S(1)} %get-tuple-element.46), channel_id=1, source_target_pairs={{0,2},{1,3},{2,0},{3,1},{4,6},{5,7},{6,4},{7,5},{8,10},{9,11},{10,... | collective-permute-start | bytes 196616 | tf_op jit(solution)/shard_map/ppermute | solution.py:29
  18.1 4.0 %collective-permute-start.5 = (bf16[128,256]{1,0:T(8,128)(2,1)S(1)}, bf16[128,256]{1,0:T(8,128)(2,1)S(1)}, u32[]{:S(2)}, u32[]{:S(2)}) collective-permute-start(bf16[128,256]{1,0:T(8,128)(2,1)S(1)} %get-tuple-element.47), channel_id=1, source_target_pairs={{0,3},{1,2},{2,1},{3,0},{4,7},{5,6},{6,5},{7,4},{8,11},{9,10},{10,... | collective-permute-start | bytes 196616 | tf_op jit(solution)/shard_map/ppermute | solution.py:29
  22.0 8.1 %copy-start = (bf16[1,2048,512]{2,1,0:T(8,128)(2,1)S(1)}, bf16[1,2048,512]{2,1,0:T(8,128)(2,1)}, u32[]{:S(2)}) copy-start(bf16[1,2048,512]{2,1,0:T(8,128)(2,1)} %param.22) | copy-start | bytes 6291460
  22.0 8.1 %copy-start.1 = (bf16[1,2048,512]{2,1,0:T(8,128)(2,1)S(1)}, bf16[1,2048,512]{2,1,0:T(8,128)(2,1)}, u32[]{:S(2)}) copy-start(bf16[1,2048,512]{2,1,0:T(8,128)(2,1)} %param.23) | copy-start | bytes 6291460
  25.2 18.8 %collective-permute-start.12 = (bf16[128,2176]{1,0:T(8,128)(2,1)S(1)}, bf16[128,2176]{1,0:T(8,128)(2,1)S(1)}, u32[]{:S(2)}, u32[]{:S(2)}) collective-permute-start(bf16[128,2176]{1,0:T(8,128)(2,1)S(1)} %get-tuple-element.71.refs_0_), channel_id=1, source_target_pairs={{0,4},{1,5},{2,6},{3,7},{4,0},{5,1},{6,2},{7,3},{8,12},{9,13},{10,... | collective-permute-start | bytes 1671176 | tf_op jit(solution)/shard_map/ppermute | solution.py:29
  27.5 15.3 %collective-permute-start.6 = (bf16[64,2176]{1,0:T(8,128)(2,1)S(1)}, bf16[64,2176]{1,0:T(8,128)(2,1)S(1)}, u32[]{:S(2)}, u32[]{:S(2)}) collective-permute-start(bf16[64,2176]{1,0:T(8,128)(2,1)S(1)} %slice.55), channel_id=1, source_target_pairs={{0,16},{1,17},{2,18},{3,19},{4,20},{5,21},{6,22},{7,23},{8,24},{9,... | collective-permute-start | bytes 835592 | tf_op jit(solution)/shard_map/ppermute | solution.py:29
  30.2 1.0 copy-start.3
  31.2 1.0 copy-start.4
  32.3 1.0 copy-start.5
  42.8 7.6 %collective-permute-start.11 = (bf16[64,2176]{1,0:T(8,128)(2,1)S(1)}, bf16[64,2176]{1,0:T(8,128)(2,1)S(1)}, u32[]{:S(2)}, u32[]{:S(2)}) collective-permute-start(bf16[64,2176]{1,0:T(8,128)(2,1)S(1)} %collective-permute-done.6.refs_0_), channel_id=1, source_target_pairs={{0,4},{1,5},{2,6},{3,7},{4,0},{5,1},{6,2},{7,3},{8,12},{9,13},{10,... | collective-permute-start | bytes 835592 | tf_op jit(solution)/shard_map/ppermute | solution.py:29
  43.3 7.5 %collective-permute-start.13 = (bf16[64,2176]{1,0:T(8,128)(2,1)S(1)}, bf16[64,2176]{1,0:T(8,128)(2,1)S(1)}, u32[]{:S(2)}, u32[]{:S(2)}) collective-permute-start(bf16[64,2176]{1,0:T(8,128)(2,1)S(1)} %collective-permute-done.6.refs_0_), channel_id=1, source_target_pairs={{0,8},{1,9},{2,10},{3,11},{4,12},{5,13},{6,14},{7,15},{8,0},{9,1},... | collective-permute-start | bytes 835592 | tf_op jit(solution)/shard_map/ppermute | solution.py:29
  50.8 6.7 %collective-permute-start.14 = (bf16[64,2176]{1,0:T(8,128)(2,1)S(1)}, bf16[64,2176]{1,0:T(8,128)(2,1)S(1)}, u32[]{:S(2)}, u32[]{:S(2)}) collective-permute-start(bf16[64,2176]{1,0:T(8,128)(2,1)S(1)} %collective-permute-done.13.refs_0_), channel_id=1, source_target_pairs={{0,4},{1,5},{2,6},{3,7},{4,0},{5,1},{6,2},{7,3},{8,12},{9,13},{10,... | collective-permute-start | bytes 835592 | tf_op jit(solution)/shard_map/ppermute | solution.py:29
  52.1 9.4 %collective-permute-start.18 = (bf16[64,2176]{1,0:T(8,128)(2,1)S(1)}, bf16[64,2176]{1,0:T(8,128)(2,1)S(1)}, u32[]{:S(2)}, u32[]{:S(2)}) collective-permute-start(bf16[64,2176]{1,0:T(8,128)(2,1)S(1)} %collective-permute-done.11.refs_1_), channel_id=1, source_target_pairs={{0,2},{1,3},{2,0},{3,1},{4,6},{5,7},{6,4},{7,5},{8,10},{9,11},{10,... | collective-permute-start | bytes 835592 | tf_op jit(solution)/shard_map/ppermute | solution.py:29
  52.1 12.3 %collective-permute-start.17 = (bf16[64,2176]{1,0:T(8,128)(2,1)S(1)}, bf16[64,2176]{1,0:T(8,128)(2,1)S(1)}, u32[]{:S(2)}, u32[]{:S(2)}) collective-permute-start(bf16[64,2176]{1,0:T(8,128)(2,1)S(1)} %collective-permute-done.6.refs_0_), channel_id=1, source_target_pairs={{0,2},{1,3},{2,0},{3,1},{4,6},{5,7},{6,4},{7,5},{8,10},{9,11},{10,... | collective-permute-start | bytes 835592 | tf_op jit(solution)/shard_map/ppermute | solution.py:29
  54.1 41.2 %collective-permute-start.23 = (bf16[128,2176]{1,0:T(8,128)(2,1)S(1)}, bf16[128,2176]{1,0:T(8,128)(2,1)S(1)}, u32[]{:S(2)}, u32[]{:S(2)}) collective-permute-start(bf16[128,2176]{1,0:T(8,128)(2,1)S(1)} %get-tuple-element.71.refs_0_), channel_id=1, source_target_pairs={{0,8},{1,9},{2,10},{3,11},{4,12},{5,13},{6,14},{7,15},{8,0},{9,1},... | collective-permute-start | bytes 1671176 | tf_op jit(solution)/shard_map/ppermute | solution.py:29
  55.8 39.5 %collective-permute-start.24 = (bf16[128,2176]{1,0:T(8,128)(2,1)S(1)}, bf16[128,2176]{1,0:T(8,128)(2,1)S(1)}, u32[]{:S(2)}, u32[]{:S(2)}) collective-permute-start(bf16[128,2176]{1,0:T(8,128)(2,1)S(1)} %collective-permute-done.12.refs_0_), channel_id=1, source_target_pairs={{0,8},{1,9},{2,10},{3,11},{4,12},{5,13},{6,14},{7,15},{8,0},{9,1},... | collective-permute-start | bytes 1671176 | tf_op jit(solution)/shard_map/ppermute | solution.py:29
  68.0 31.5 %collective-permute-start.22 = (bf16[128,2048]{1,0:T(8,128)(2,1)S(1)}, bf16[128,2048]{1,0:T(8,128)(2,1)S(1)}, u32[]{:S(2)}, u32[]{:S(2)}) collective-permute-start(bf16[128,2048]{1,0:T(8,128)(2,1)S(1)} %get-tuple-element.68), channel_id=1, source_target_pairs={{0,2},{1,3},{2,0},{3,1},{4,6},{5,7},{6,4},{7,5},{8,10},{9,11},{10,... | collective-permute-start | bytes 1572872 | tf_op jit(solution)/shard_map/ppermute | solution.py:29
  68.3 19.4 %collective-permute-start.20 = (bf16[64,2176]{1,0:T(8,128)(2,1)S(1)}, bf16[64,2176]{1,0:T(8,128)(2,1)S(1)}, u32[]{:S(2)}, u32[]{:S(2)}) collective-permute-start(bf16[64,2176]{1,0:T(8,128)(2,1)S(1)} %collective-permute-done.14.refs_2_), channel_id=1, source_target_pairs={{0,2},{1,3},{2,0},{3,1},{4,6},{5,7},{6,4},{7,5},{8,10},{9,11},{10,... | collective-permute-start | bytes 835592 | tf_op jit(solution)/shard_map/ppermute | solution.py:29
  70.1 20.7 %collective-permute-start.19 = (bf16[64,2176]{1,0:T(8,128)(2,1)S(1)}, bf16[64,2176]{1,0:T(8,128)(2,1)S(1)}, u32[]{:S(2)}, u32[]{:S(2)}) collective-permute-start(bf16[64,2176]{1,0:T(8,128)(2,1)S(1)} %collective-permute-done.13.refs_0_), channel_id=1, source_target_pairs={{0,2},{1,3},{2,0},{3,1},{4,6},{5,7},{6,4},{7,5},{8,10},{9,11},{10,... | collective-permute-start | bytes 835592 | tf_op jit(solution)/shard_map/ppermute | solution.py:29
  87.8 13.1 %collective-permute-start.15 = (bf16[128,2048]{1,0:T(8,128)(2,1)S(1)}, bf16[128,2048]{1,0:T(8,128)(2,1)S(1)}, u32[]{:S(2)}, u32[]{:S(2)}) collective-permute-start(bf16[128,2048]{1,0:T(8,128)(2,1)S(1)} %shard_map.139), channel_id=1, source_target_pairs={{0,4},{1,5},{2,6},{3,7},{4,0},{5,1},{6,2},{7,3},{8,12},{9,13},{10,... | collective-permute-start | bytes 1572872 | tf_op jit(solution)/shard_map/ppermute | solution.py:29
  94.5 16.5 %collective-permute-start.21 = (bf16[128,2048]{1,0:T(8,128)(2,1)S(1)}, bf16[128,2048]{1,0:T(8,128)(2,1)S(1)}, u32[]{:S(2)}, u32[]{:S(2)}) collective-permute-start(bf16[128,2048]{1,0:T(8,128)(2,1)S(1)} %get-tuple-element.70), channel_id=1, source_target_pairs={{0,4},{1,5},{2,6},{3,7},{4,0},{5,1},{6,2},{7,3},{8,12},{9,13},{10,... | collective-permute-start | bytes 1572872 | tf_op jit(solution)/shard_map/ppermute | solution.py:29
  98.9 21.0 %collective-permute-start.29 = (bf16[128,2048]{1,0:T(8,128)(2,1)S(1)}, bf16[128,2048]{1,0:T(8,128)(2,1)S(1)}, u32[]{:S(2)}, u32[]{:S(2)}) collective-permute-start(bf16[128,2048]{1,0:T(8,128)(2,1)S(1)} %get-tuple-element.73), channel_id=1, source_target_pairs={{0,2},{1,3},{2,0},{3,1},{4,6},{5,7},{6,4},{7,5},{8,10},{9,11},{10,... | collective-permute-start | bytes 1572872 | tf_op jit(solution)/shard_map/ppermute | solution.py:29
  99.6 14.2 %collective-permute-start.25 = (bf16[64,2048]{1,0:T(8,128)(2,1)S(1)}, bf16[64,2048]{1,0:T(8,128)(2,1)S(1)}, u32[]{:S(2)}, u32[]{:S(2)}) collective-permute-start(bf16[64,2048]{1,0:T(8,128)(2,1)S(1)} %add_convert_fusion.6), channel_id=1, source_target_pairs={{0,4},{1,5},{2,6},{3,7},{4,0},{5,1},{6,2},{7,3},{8,12},{9,13},{10,... | collective-permute-start | bytes 786440 | tf_op jit(solution)/shard_map/ppermute | solution.py:29
  101.0 26.9 %collective-permute-start.16 = (bf16[64,2048]{1,0:T(8,128)(2,1)S(1)}, bf16[64,2048]{1,0:T(8,128)(2,1)S(1)}, u32[]{:S(2)}, u32[]{:S(2)}) collective-permute-start(bf16[64,2048]{1,0:T(8,128)(2,1)S(1)} %get-tuple-element.81), channel_id=1, source_target_pairs={{0,2},{1,3},{2,0},{3,1},{4,6},{5,7},{6,4},{7,5},{8,10},{9,11},{10,... | collective-permute-start | bytes 786440 | tf_op jit(solution)/shard_map/ppermute | solution.py:29
  113.9 19.3 %collective-permute-start.26 = (bf16[64,2048]{1,0:T(8,128)(2,1)S(1)}, bf16[64,2048]{1,0:T(8,128)(2,1)S(1)}, u32[]{:S(2)}, u32[]{:S(2)}) collective-permute-start(bf16[64,2048]{1,0:T(8,128)(2,1)S(1)} %add_convert_fusion.5), channel_id=1, source_target_pairs={{0,16},{1,17},{2,18},{3,19},{4,20},{5,21},{6,22},{7,23},{8,24},{9,... | collective-permute-start | bytes 786440 | tf_op jit(solution)/shard_map/ppermute | solution.py:29
  119.5 6.4 %collective-permute-start.27 = (bf16[64,2048]{1,0:T(8,128)(2,1)S(1)}, bf16[64,2048]{1,0:T(8,128)(2,1)S(1)}, u32[]{:S(2)}, u32[]{:S(2)}) collective-permute-start(bf16[64,2048]{1,0:T(8,128)(2,1)S(1)} %add_convert_fusion.4), channel_id=1, source_target_pairs={{0,2},{1,3},{2,0},{3,1},{4,6},{5,7},{6,4},{7,5},{8,10},{9,11},{10,... | collective-permute-start | bytes 786440 | tf_op jit(solution)/shard_map/ppermute | solution.py:29
  119.9 6.9 %collective-permute-start.30 = (bf16[64,2048]{1,0:T(8,128)(2,1)S(1)}, bf16[64,2048]{1,0:T(8,128)(2,1)S(1)}, u32[]{:S(2)}, u32[]{:S(2)}) collective-permute-start(bf16[64,2048]{1,0:T(8,128)(2,1)S(1)} %add_convert_fusion.2), channel_id=1, source_target_pairs={{0,4},{1,5},{2,6},{3,7},{4,0},{5,1},{6,2},{7,3},{8,12},{9,13},{10,... | collective-permute-start | bytes 786440 | tf_op jit(solution)/shard_map/ppermute | solution.py:29
  126.0 9.5 %collective-permute-start.28 = (bf16[64,2048]{1,0:T(8,128)(2,1)S(1)}, bf16[64,2048]{1,0:T(8,128)(2,1)S(1)}, u32[]{:S(2)}, u32[]{:S(2)}) collective-permute-start(bf16[64,2048]{1,0:T(8,128)(2,1)S(1)} %add_convert_fusion.3), channel_id=1, source_target_pairs={{0,24},{1,25},{2,26},{3,27},{4,28},{5,29},{6,30},{7,31},{8,16},{9,... | collective-permute-start | bytes 786440 | tf_op jit(solution)/shard_map/ppermute | solution.py:29
  126.9 13.4 %collective-permute-start.31 = (bf16[64,2048]{1,0:T(8,128)(2,1)S(1)}, bf16[64,2048]{1,0:T(8,128)(2,1)S(1)}, u32[]{:S(2)}, u32[]{:S(2)}) collective-permute-start(bf16[64,2048]{1,0:T(8,128)(2,1)S(1)} %add_convert_fusion.1), channel_id=1, source_target_pairs={{0,8},{1,9},{2,10},{3,11},{4,12},{5,13},{6,14},{7,15},{8,0},{9,1},... | collective-permute-start | bytes 786440 | tf_op jit(solution)/shard_map/ppermute | solution.py:29

commit v2 on v1

--- a/solution.py
+++ b/solution.py
@@ -380,11 +380,10 @@
         ],
         compiler_params=pltpu.CompilerParams(vmem_limit_bytes=4 * MIB),
     )
-    rim_rows, weights[1], weights[3] = tied(rim_rows, weights[1], weights[3])
     groups = pool(rim_rows, *kept_in_hbm(pooled_in, pool_weight, pool_scale[None]))
     groups = [swapped(group, flip) if flip else group for flip, group in enumerate(groups)]
     depth = out_weight.shape[0] // tp_size
-    pair, own_resid = pl.pallas_call(
+    norm = pl.pallas_call(
         norm_kernel,
         out_shape=[
             jax.ShapeDtypeStruct((2 * rows, width + lanes), bf16),
@@ -403,7 +402,8 @@
             pltpu.SemaphoreType.DMA((tp_size + 5,)),
         ],
         compiler_params=pltpu.CompilerParams(vmem_limit_bytes=10 * MIB),
-    )(
+    )
+    pair, own_resid = norm(
         *groups,
         *kept_in_hbm(routes.T, route_weights.T, stream, out_weight, norm_gain[None]),
     )

time: 141 us -> 140 us (level)
  waiting for transfers between devices: 78.5 us -> 76.5 us
    ppermute x31, waiting for transfers between devices: 77.2 us -> 75.1 us  [swapped(): lax.ppermute(value, AXES, [(source, source ^ flip) for source in range(co...]
where the time goes in v2:
time: 140 us
  waiting for transfers between devices  76.5 us (55%)
  starting transfers between devices  38.1 us (27%)
  Pallas kernels  19.9 us (14%)
  local copies, waits for them, and re-layouts  3.85 us (3%)
  other arithmetic  1.55 us (1%)
    ppermute x31, waiting for transfers between devices, swapped(): lax.ppermute(value, AXES, [(source, source ^ flip) for source in range(co...  75.1 us
    ppermute x31, starting transfers between devices, swapped(): lax.ppermute(value, AXES, [(source, source ^ flip) for source in range(co...  33.2 us
    pallas_call x5, Pallas kernels, run_expert(): pl.pallas_call(functools.partial(expert_kernel, len(pieces), tuple(takes)...  15.3 us
    ppermute x1, starting transfers between devices, passed_along(): lax.ppermute(value, axis, [(source, source + steps) for source in range(i...  4.89 us
    unnamed x12, local copies, waits for them, and re-layouts  3.13 us
    pallas_call x1, Pallas kernels, dense_plan(): norm(*groups, *kept_in_hbm(routes.T, route_weights.T, stream, out_weight,...  3.1 us
  transfers between devices with their start and end apart: 32, of which 18 were waited for; matrix products, arithmetic and copies ran while one was open for 1% of the time, Pallas kernels for 14%

profile of v2, /device:TPU:0, one launch (start us, length us, event | category | flops | bytes accessed | tf_op | source)
XLA Modules:
  0.0 140.1 jit_solution(17494687291788023917)
XLA Ops:
  0.0 0.5 collective-permute-start.5
  0.5 0.5 collective-permute-start.7
  1.0 0.7 slice.54
  1.7 4.9 %collective-permute-start = (bf16[16,256]{1,0:T(8,128)(2,1)S(1)}, bf16[16,256]{1,0:T(8,128)(2,1)S(1)}, u32[]{:S(2)}, u32[]{:S(2)}) collective-permute-start(bf16[16,256]{1,0:T(8,128)(2,1)S(1)} %slice.54), channel_id=1, source_target_pairs={{0,4},{4,8},{8,12},{12,16},{16,20},{20,24},{24,28},{1,5},{5,9},{9,... | collective-permute-start | bytes 24584 | tf_op jit(solution)/shard_map/ppermute | solution.py:24
  6.6 1.3 collective-permute-done.rim_ref
  8.0 1.5 %shard_map.136 = (bf16[128,256]{1,0:T(8,128)(2,1)S(1)}, bf16[128,256]{1,0:T(8,128)(2,1)S(1)}, bf16[128,256]{1,0:T(8,128)(2,1)S(1)}, bf16[128,256]{1,0:T(8,128)(2,1)S(1)}) custom-call(bf16[16,256]{1,0:T(8,128)(2,1)S(1)} %collective-permute-done.rim_ref, bf16[256,256]{1,0:T(8,128)(2,1)} %pooled_hbm.1, bf16[1,256,256]{2,1,0:T(8,128)(2,1)} %weight_hbm.1, ...), custom_call_target="tpu_custom_call" | custom-call | tf_op jit(solution)/shard_map/pallas_call | solution.py:383
  9.5 0.1 collective-permute-start.1
  9.5 1.8 %collective-permute-done.1.refs_1_ = bf16[128,256]{1,0:T(8,128)(2,1)S(1)} collective-permute-done((bf16[128,256]{1,0:T(8,128)(2,1)S(1)}, bf16[128,256]{1,0:T(8,128)(2,1)S(1)}, u32[]{:S(2)}, u32[]{:S(2)}) %collective-permute-start.1) | collective-permute-done | bytes 65568 | tf_op jit(solution)/shard_map/ppermute | solution.py:29
  11.3 2.8 %collective-permute-start.2 = (bf16[128,256]{1,0:T(8,128)(2,1)S(1)}, bf16[128,256]{1,0:T(8,128)(2,1)S(1)}, u32[]{:S(2)}, u32[]{:S(2)}) collective-permute-start(bf16[128,256]{1,0:T(8,128)(2,1)S(1)} %get-tuple-element.42), channel_id=1, source_target_pairs={{0,2},{1,3},{2,0},{3,1},{4,6},{5,7},{6,4},{7,5},{8,10},{9,11},{10,... | collective-permute-start | bytes 196616 | tf_op jit(solution)/shard_map/ppermute | solution.py:29
  14.2 2.4 %collective-permute-done.2.refs_2_ = bf16[128,256]{1,0:T(8,128)(2,1)S(1)} collective-permute-done((bf16[128,256]{1,0:T(8,128)(2,1)S(1)}, bf16[128,256]{1,0:T(8,128)(2,1)S(1)}, u32[]{:S(2)}, u32[]{:S(2)}) %collective-permute-start.2) | collective-permute-done | bytes 65568 | tf_op jit(solution)/shard_map/ppermute | solution.py:29
  16.6 0.5 collective-permute-start.3
  17.0 3.5 %collective-permute-done.3.refs_3_ = bf16[128,256]{1,0:T(8,128)(2,1)S(1)} collective-permute-done((bf16[128,256]{1,0:T(8,128)(2,1)S(1)}, bf16[128,256]{1,0:T(8,128)(2,1)S(1)}, u32[]{:S(2)}, u32[]{:S(2)}) %collective-permute-start.3) | collective-permute-done | bytes 65568 | tf_op jit(solution)/shard_map/ppermute | solution.py:29
  20.5 0.2 collective-permute-start.8
  20.8 0.3 collective-permute-start.9
  21.1 3.1 %shard_map.137 = (bf16[128,2176]{1,0:T(8,128)(2,1)S(1)}, bf16[64,2048]{1,0:T(8,128)(2,1)S(1)}) custom-call(bf16[128,256]{1,0:T(8,128)(2,1)S(1)} %get-tuple-element.40.refs_0_, bf16[128,256]{1,0:T(8,128)(2,1)S(1)} %collective-permute-done.1.refs_1_, bf16[128,256]{1,0:T(8,128)(2,1)S(1)} %collective-permute-done.2.refs_2_, ...), custom_call_target="tpu_custom_call" | custom-call | tf_op jit(solution)/shard_map/pallas_call | solution.py:406
  24.2 2.4 %collective-permute-start.12 = (bf16[128,2176]{1,0:T(8,128)(2,1)S(1)}, bf16[128,2176]{1,0:T(8,128)(2,1)S(1)}, u32[]{:S(2)}, u32[]{:S(2)}) collective-permute-start(bf16[128,2176]{1,0:T(8,128)(2,1)S(1)} %get-tuple-element.65.refs_0_), channel_id=1, source_target_pairs={{0,4},{1,5},{2,6},{3,7},{4,0},{5,1},{6,2},{7,3},{8,12},{9,13},{10,... | collective-permute-start | bytes 1671176 | tf_op jit(solution)/shard_map/ppermute | solution.py:29
  26.6 2.6 %collective-permute-start.4 = (bf16[64,2176]{1,0:T(8,128)(2,1)S(1)}, bf16[64,2176]{1,0:T(8,128)(2,1)S(1)}, u32[]{:S(2)}, u32[]{:S(2)}) collective-permute-start(bf16[64,2176]{1,0:T(8,128)(2,1)S(1)} %slice.55), channel_id=1, source_target_pairs={{0,16},{1,17},{2,18},{3,19},{4,20},{5,21},{6,22},{7,23},{8,24},{9,... | collective-permute-start | bytes 835592 | tf_op jit(solution)/shard_map/ppermute | solution.py:29
  29.2 1.0 copy-done.3
  30.2 1.0 copy-done.4
  31.3 1.0 copy-done.5
  32.3 2.6 %shard_map.138 = bf16[128,2048]{1,0:T(8,128)(2,1)S(1)} custom-call(bf16[128,2176]{1,0:T(8,128)(2,1)S(1)} %get-tuple-element.65.refs_0_, bf16[2048,512]{1,0:T(8,128)(2,1)S(1)} %bitcast.8, bf16[2048,512]{1,0:T(8,128)(2,1)S(1)} %collective-permute-done.5.refs_2_.refs_6_.refs_3_, bf16[2048,512]{1,0:T(8,128)(2,1)S(1)} %bitcast.14, ...), custom_call_target="tpu_custom_call" | custom-call | tf_op jit(solution)/shard_map/pallas_call | solution.py:328
  35.0 6.9 %collective-permute-done.4.refs_0_ = bf16[64,2176]{1,0:T(8,128)(2,1)S(1)} collective-permute-done((bf16[64,2176]{1,0:T(8,128)(2,1)S(1)}, bf16[64,2176]{1,0:T(8,128)(2,1)S(1)}, u32[]{:S(2)}, u32[]{:S(2)}) %collective-permute-start.4) | collective-permute-done | bytes 278560 | tf_op jit(solution)/shard_map/ppermute | solution.py:29
  41.8 0.5 collective-permute-start.11
  42.3 0.7 collective-permute-start.13
  43.0 1.9 %shard_map.139 = bf16[128,2048]{1,0:T(8,128)(2,1)S(1)} custom-call(bf16[128,2176]{1,0:T(8,128)(2,1)S(1)} %collective-permute-done.12.refs_0_, bf16[2048,512]{1,0:T(8,128)(2,1)S(1)} %bitcast.9, bf16[2048,512]{1,0:T(8,128)(2,1)S(1)} %collective-permute-done.5.refs_2_.refs_6_.refs_3_, bf16[2048,512]{1,0:T(8,128)(2,1)S(1)} %bitcast.15, ...), custom_call_target="tpu_custom_call" | custom-call | tf_op jit(solution)/shard_map/pallas_call | solution.py:328
  44.9 4.5 %collective-permute-done.11.refs_1_ = bf16[64,2176]{1,0:T(8,128)(2,1)S(1)} collective-permute-done((bf16[64,2176]{1,0:T(8,128)(2,1)S(1)}, bf16[64,2176]{1,0:T(8,128)(2,1)S(1)}, u32[]{:S(2)}, u32[]{:S(2)}) %collective-permute-start.11) | collective-permute-done | bytes 278560 | tf_op jit(solution)/shard_map/ppermute | solution.py:29
  49.4 0.4 collective-permute-done.13.refs_0_
  49.8 1.3 collective-permute-start.14
  51.1 0.7 collective-permute-start.18
  51.9 1.3 collective-permute-start.17
  53.2 1.7 %collective-permute-start.23 = (bf16[128,2176]{1,0:T(8,128)(2,1)S(1)}, bf16[128,2176]{1,0:T(8,128)(2,1)S(1)}, u32[]{:S(2)}, u32[]{:S(2)}) collective-permute-start(bf16[128,2176]{1,0:T(8,128)(2,1)S(1)} %get-tuple-element.65.refs_0_), channel_id=1, source_target_pairs={{0,8},{1,9},{2,10},{3,11},{4,12},{5,13},{6,14},{7,15},{8,0},{9,1},... | collective-permute-start | bytes 1671176 | tf_op jit(solution)/shard_map/ppermute | solution.py:29
  54.8 0.3 collective-permute-start.24
  55.2 1.3 collective-permute-done.14.refs_2_
  56.5 4.0 %collective-permute-done.18.refs_3_ = bf16[64,2176]{1,0:T(8,128)(2,1)S(1)} collective-permute-done((bf16[64,2176]{1,0:T(8,128)(2,1)S(1)}, bf16[64,2176]{1,0:T(8,128)(2,1)S(1)}, u32[]{:S(2)}, u32[]{:S(2)}) %collective-permute-start.18) | collective-permute-done | bytes 278560 | tf_op jit(solution)/shard_map/ppermute | solution.py:29
  60.5 3.0 %collective-permute-done.17.refs_2_ = bf16[64,2176]{1,0:T(8,128)(2,1)S(1)} collective-permute-done((bf16[64,2176]{1,0:T(8,128)(2,1)S(1)}, bf16[64,2176]{1,0:T(8,128)(2,1)S(1)}, u32[]{:S(2)}, u32[]{:S(2)}) %collective-permute-start.17) | collective-permute-done | bytes 278560 | tf_op jit(solution)/shard_map/ppermute | solution.py:29
  63.5 3.5 %shard_map.143 = (bf16[128,2048]{1,0:T(8,128)(2,1)S(1)}, bf16[128,2048]{1,0:T(8,128)(2,1)S(1)}) custom-call(bf16[64,2176]{1,0:T(8,128)(2,1)S(1)} %collective-permute-done.4.refs_0_, bf16[64,2176]{1,0:T(8,128)(2,1)S(1)} %collective-permute-done.11.refs_1_, bf16[64,2176]{1,0:T(8,128)(2,1)S(1)} %collective-permute-done.17.refs_2_, ...), custom_call_target="tpu_custom_call" | custom-call | tf_op jit(solution)/shard_map/pallas_call | solution.py:328
  67.0 0.8 collective-permute-start.22
  67.8 1.3 collective-permute-start.20
  69.1 0.7 collective-permute-start.19
  69.8 17.0 %collective-permute-done.20.refs_3_ = bf16[64,2176]{1,0:T(8,128)(2,1)S(1)} collective-permute-done((bf16[64,2176]{1,0:T(8,128)(2,1)S(1)}, bf16[64,2176]{1,0:T(8,128)(2,1)S(1)}, u32[]{:S(2)}, u32[]{:S(2)}) %collective-permute-start.20) | collective-permute-done | bytes 278560 | tf_op jit(solution)/shard_map/ppermute | solution.py:29
  86.8 0.8 collective-permute-start.15
  87.6 2.1 %collective-permute-done.19.refs_1_ = bf16[64,2176]{1,0:T(8,128)(2,1)S(1)} collective-permute-done((bf16[64,2176]{1,0:T(8,128)(2,1)S(1)}, bf16[64,2176]{1,0:T(8,128)(2,1)S(1)}, u32[]{:S(2)}, u32[]{:S(2)}) %collective-permute-start.19) | collective-permute-done | bytes 278560 | tf_op jit(solution)/shard_map/ppermute | solution.py:29
  89.8 3.7 %shard_map.145 = (bf16[128,2048]{1,0:T(8,128)(2,1)S(1)}, bf16[128,2048]{1,0:T(8,128)(2,1)S(1)}) custom-call(bf16[64,2176]{1,0:T(8,128)(2,1)S(1)} %collective-permute-done.13.refs_0_, bf16[64,2176]{1,0:T(8,128)(2,1)S(1)} %collective-permute-done.19.refs_1_, bf16[64,2176]{1,0:T(8,128)(2,1)S(1)} %collective-permute-done.14.refs_2_, ...), custom_call_target="tpu_custom_call" | custom-call | tf_op jit(solution)/shard_map/pallas_call | solution.py:328
  93.5 0.8 collective-permute-start.21
  94.4 3.5 %shard_map.146 = (bf16[128,2048]{1,0:T(8,128)(2,1)S(1)}, bf16[128,2048]{1,0:T(8,128)(2,1)S(1)}) custom-call(bf16[128,2176]{1,0:T(8,128)(2,1)S(1)} %collective-permute-done.23.refs_0_, bf16[128,2176]{1,0:T(8,128)(2,1)S(1)} %collective-permute-done.24.refs_1_, bf16[2048,512]{1,0:T(8,128)(2,1)S(1)} %bitcast.12, ...), custom_call_target="tpu_custom_call" | custom-call | tf_op jit(solution)/shard_map/pallas_call | solution.py:328
  97.9 0.5 collective-permute-start.29
  98.5 1.6 %collective-permute-start.25 = (bf16[64,2048]{1,0:T(8,128)(2,1)S(1)}, bf16[64,2048]{1,0:T(8,128)(2,1)S(1)}, u32[]{:S(2)}, u32[]{:S(2)}) collective-permute-start(bf16[64,2048]{1,0:T(8,128)(2,1)S(1)} %add_convert_fusion.6), channel_id=1, source_target_pairs={{0,4},{1,5},{2,6},{3,7},{4,0},{5,1},{6,2},{7,3},{8,12},{9,13},{10,... | collective-permute-start | bytes 786440 | tf_op jit(solution)/shard_map/ppermute | solution.py:29
  100.1 0.2 add_convert_fusion.7
  100.2 1.4 collective-permute-start.16
  101.6 8.4 %collective-permute-done.21 = bf16[128,2048]{1,0:T(8,128)(2,1)S(1)} collective-permute-done((bf16[128,2048]{1,0:T(8,128)(2,1)S(1)}, bf16[128,2048]{1,0:T(8,128)(2,1)S(1)}, u32[]{:S(2)}, u32[]{:S(2)}) %collective-permute-start.21) | collective-permute-done | bytes 524320 | tf_op jit(solution)/shard_map/ppermute | solution.py:29
  110.0 2.8 %collective-permute-done.25 = bf16[64,2048]{1,0:T(8,128)(2,1)S(1)} collective-permute-done((bf16[64,2048]{1,0:T(8,128)(2,1)S(1)}, bf16[64,2048]{1,0:T(8,128)(2,1)S(1)}, u32[]{:S(2)}, u32[]{:S(2)}) %collective-permute-start.25) | collective-permute-done | bytes 262176 | tf_op jit(solution)/shard_map/ppermute | solution.py:29
  112.8 0.1 add_convert_fusion.5
  112.9 5.5 %collective-permute-start.26 = (bf16[64,2048]{1,0:T(8,128)(2,1)S(1)}, bf16[64,2048]{1,0:T(8,128)(2,1)S(1)}, u32[]{:S(2)}, u32[]{:S(2)}) collective-permute-start(bf16[64,2048]{1,0:T(8,128)(2,1)S(1)} %add_convert_fusion.5), channel_id=1, source_target_pairs={{0,16},{1,17},{2,18},{3,19},{4,20},{5,21},{6,22},{7,23},{8,24},{9,... | collective-permute-start | bytes 786440 | tf_op jit(solution)/shard_map/ppermute | solution.py:29
  118.5 0.8 collective-permute-start.27
  119.4 0.6 collective-permute-start.30
  119.9 5.0 %collective-permute-done.27 = bf16[64,2048]{1,0:T(8,128)(2,1)S(1)} collective-permute-done((bf16[64,2048]{1,0:T(8,128)(2,1)S(1)}, bf16[64,2048]{1,0:T(8,128)(2,1)S(1)}, u32[]{:S(2)}, u32[]{:S(2)}) %collective-permute-start.27) | collective-permute-done | bytes 262176 | tf_op jit(solution)/shard_map/ppermute | solution.py:29
  124.9 0.1 add_convert_fusion.3
  125.0 0.8 collective-permute-start.28
  125.8 0.1 add_convert_fusion.1
  125.9 1.3 collective-permute-start.31
  127.2 5.0 %collective-permute-done.26 = bf16[64,2048]{1,0:T(8,128)(2,1)S(1)} collective-permute-done((bf16[64,2048]{1,0:T(8,128)(2,1)S(1)}, bf16[64,2048]{1,0:T(8,128)(2,1)S(1)}, u32[]{:S(2)}, u32[]{:S(2)}) %collective-permute-start.26) | collective-permute-done | bytes 262176 | tf_op jit(solution)/shard_map/ppermute | solution.py:29
  132.2 2.3 %collective-permute-done.28 = bf16[64,2048]{1,0:T(8,128)(2,1)S(1)} collective-permute-done((bf16[64,2048]{1,0:T(8,128)(2,1)S(1)}, bf16[64,2048]{1,0:T(8,128)(2,1)S(1)}, u32[]{:S(2)}, u32[]{:S(2)}) %collective-permute-start.28) | collective-permute-done | bytes 262176 | tf_op jit(solution)/shard_map/ppermute | solution.py:29
  134.5 4.8 %collective-permute-done.31 = bf16[64,2048]{1,0:T(8,128)(2,1)S(1)} collective-permute-done((bf16[64,2048]{1,0:T(8,128)(2,1)S(1)}, bf16[64,2048]{1,0:T(8,128)(2,1)S(1)}, u32[]{:S(2)}, u32[]{:S(2)}) %collective-permute-start.31) | collective-permute-done | bytes 262176 | tf_op jit(solution)/shard_map/ppermute | solution.py:29
  139.3 0.9 add_convert_fusion
  (35 shorter events, 0.4 us)
Async XLA Ops:
  0.0 29.1 %collective-permute-start.5 = (bf16[2048,512]{1,0:T(8,128)(2,1)}, bf16[2048,512]{1,0:T(8,128)(2,1)S(1)}, u32[]{:S(2)}, u32[]{:S(2)}) collective-permute-start(bf16[2048,512]{1,0:T(8,128)(2,1)} %bitcast.7), channel_id=1, source_target_pairs={{0,1},{1,0},{2,3},{3,2},{4,5},{5,4},{6,7},{7,6},{8,9},{9,8},{10,11... | collective-permute-start | bytes 6291464 | tf_op jit(solution)/shard_map/ppermute | solution.py:29
  0.5 28.7 %collective-permute-start.6 = (bf16[2048,512]{1,0:T(8,128)(2,1)}, bf16[2048,512]{1,0:T(8,128)(2,1)S(1)}, u32[]{:S(2)}, u32[]{:S(2)}) collective-permute-start(bf16[2048,512]{1,0:T(8,128)(2,1)} %bitcast.13), channel_id=1, source_target_pairs={{0,1},{1,0},{2,3},{3,2},{4,5},{5,4},{6,7},{7,6},{8,9},{9,8},{10,11... | collective-permute-start | bytes 6291464 | tf_op jit(solution)/shard_map/ppermute | solution.py:29
  0.5 28.6 %collective-permute-start.7 = (bf16[512,2048]{1,0:T(8,128)(2,1)}, bf16[512,2048]{1,0:T(8,128)(2,1)S(1)}, u32[]{:S(2)}, u32[]{:S(2)}) collective-permute-start(bf16[512,2048]{1,0:T(8,128)(2,1)} %bitcast.19), channel_id=1, source_target_pairs={{0,1},{1,0},{2,3},{3,2},{4,5},{5,4},{6,7},{7,6},{8,9},{9,8},{10,11... | collective-permute-start | bytes 6291464 | tf_op jit(solution)/shard_map/ppermute | solution.py:29
  1.0 19.8 %collective-permute-start.10 = (bf16[128,2048]{1,0:T(8,128)(2,1)}, bf16[128,2048]{1,0:T(8,128)(2,1)S(1)}, u32[]{:S(2)}, u32[]{:S(2)}) collective-permute-start(bf16[128,2048]{1,0:T(8,128)(2,1)} %refs_11_.1), channel_id=1, source_target_pairs={{0,1},{1,0},{2,3},{3,2},{4,5},{5,4},{6,7},{7,6},{8,9},{9,8},{10,11... | collective-permute-start | bytes 1572872 | tf_op jit(solution)/shard_map/ppermute | solution.py:29
  1.7 6.2 %collective-permute-start = (bf16[16,256]{1,0:T(8,128)(2,1)S(1)}, bf16[16,256]{1,0:T(8,128)(2,1)S(1)}, u32[]{:S(2)}, u32[]{:S(2)}) collective-permute-start(bf16[16,256]{1,0:T(8,128)(2,1)S(1)} %slice.54), channel_id=1, source_target_pairs={{0,4},{4,8},{8,12},{12,16},{16,20},{20,24},{24,28},{1,5},{5,9},{9,... | collective-permute-start | bytes 24584 | tf_op jit(solution)/shard_map/ppermute | solution.py:24
  8.0 21.2 %copy-start.2 = (bf16[1,512,2048]{2,1,0:T(8,128)(2,1)S(1)}, bf16[1,512,2048]{2,1,0:T(8,128)(2,1)}, u32[]{:S(2)}) copy-start(bf16[1,512,2048]{2,1,0:T(8,128)(2,1)} %param.24) | copy-start | bytes 6291460
  9.5 1.9 %collective-permute-start.1 = (bf16[128,256]{1,0:T(8,128)(2,1)S(1)}, bf16[128,256]{1,0:T(8,128)(2,1)S(1)}, u32[]{:S(2)}, u32[]{:S(2)}) collective-permute-start(bf16[128,256]{1,0:T(8,128)(2,1)S(1)} %get-tuple-element.41), channel_id=1, source_target_pairs={{0,1},{1,0},{2,3},{3,2},{4,5},{5,4},{6,7},{7,6},{8,9},{9,8},{10,11... | collective-permute-start | bytes 196616 | tf_op jit(solution)/shard_map/ppermute | solution.py:29
  11.3 5.2 %collective-permute-start.2 = (bf16[128,256]{1,0:T(8,128)(2,1)S(1)}, bf16[128,256]{1,0:T(8,128)(2,1)S(1)}, u32[]{:S(2)}, u32[]{:S(2)}) collective-permute-start(bf16[128,256]{1,0:T(8,128)(2,1)S(1)} %get-tuple-element.42), channel_id=1, source_target_pairs={{0,2},{1,3},{2,0},{3,1},{4,6},{5,7},{6,4},{7,5},{8,10},{9,11},{10,... | collective-permute-start | bytes 196616 | tf_op jit(solution)/shard_map/ppermute | solution.py:29
  16.6 4.0 %collective-permute-start.3 = (bf16[128,256]{1,0:T(8,128)(2,1)S(1)}, bf16[128,256]{1,0:T(8,128)(2,1)S(1)}, u32[]{:S(2)}, u32[]{:S(2)}) collective-permute-start(bf16[128,256]{1,0:T(8,128)(2,1)S(1)} %get-tuple-element.43), channel_id=1, source_target_pairs={{0,3},{1,2},{2,1},{3,0},{4,7},{5,6},{6,5},{7,4},{8,11},{9,10},{10,... | collective-permute-start | bytes 196616 | tf_op jit(solution)/shard_map/ppermute | solution.py:29
  20.5 3.7 %collective-permute-start.8 = (bf16[2048,128]{1,0:T(8,128)(2,1)}, bf16[2048,128]{1,0:T(8,128)(2,1)S(1)}, u32[]{:S(2)}, u32[]{:S(2)}) collective-permute-start(bf16[2048,128]{1,0:T(8,128)(2,1)} %refs_7_.3), channel_id=1, source_target_pairs={{0,1},{1,0},{2,3},{3,2},{4,5},{5,4},{6,7},{7,6},{8,9},{9,8},{10,11... | collective-permute-start | bytes 1572872 | tf_op jit(solution)/shard_map/ppermute | solution.py:29
  20.8 5.8 %collective-permute-start.9 = (bf16[2048,128]{1,0:T(8,128)(2,1)}, bf16[2048,128]{1,0:T(8,128)(2,1)S(1)}, u32[]{:S(2)}, u32[]{:S(2)}) collective-permute-start(bf16[2048,128]{1,0:T(8,128)(2,1)} %refs_9_.1), channel_id=1, source_target_pairs={{0,1},{1,0},{2,3},{3,2},{4,5},{5,4},{6,7},{7,6},{8,9},{9,8},{10,11... | collective-permute-start | bytes 1572872 | tf_op jit(solution)/shard_map/ppermute | solution.py:29
  21.1 8.1 %copy-start = (bf16[1,2048,512]{2,1,0:T(8,128)(2,1)S(1)}, bf16[1,2048,512]{2,1,0:T(8,128)(2,1)}, u32[]{:S(2)}) copy-start(bf16[1,2048,512]{2,1,0:T(8,128)(2,1)} %param.22) | copy-start | bytes 6291460
  21.1 8.1 %copy-start.1 = (bf16[1,2048,512]{2,1,0:T(8,128)(2,1)S(1)}, bf16[1,2048,512]{2,1,0:T(8,128)(2,1)}, u32[]{:S(2)}) copy-start(bf16[1,2048,512]{2,1,0:T(8,128)(2,1)} %param.23) | copy-start | bytes 6291460
  24.2 18.8 %collective-permute-start.12 = (bf16[128,2176]{1,0:T(8,128)(2,1)S(1)}, bf16[128,2176]{1,0:T(8,128)(2,1)S(1)}, u32[]{:S(2)}, u32[]{:S(2)}) collective-permute-start(bf16[128,2176]{1,0:T(8,128)(2,1)S(1)} %get-tuple-element.65.refs_0_), channel_id=1, source_target_pairs={{0,4},{1,5},{2,6},{3,7},{4,0},{5,1},{6,2},{7,3},{8,12},{9,13},{10,... | collective-permute-start | bytes 1671176 | tf_op jit(solution)/shard_map/ppermute | solution.py:29
  26.6 15.3 %collective-permute-start.4 = (bf16[64,2176]{1,0:T(8,128)(2,1)S(1)}, bf16[64,2176]{1,0:T(8,128)(2,1)S(1)}, u32[]{:S(2)}, u32[]{:S(2)}) collective-permute-start(bf16[64,2176]{1,0:T(8,128)(2,1)S(1)} %slice.55), channel_id=1, source_target_pairs={{0,16},{1,17},{2,18},{3,19},{4,20},{5,21},{6,22},{7,23},{8,24},{9,... | collective-permute-start | bytes 835592 | tf_op jit(solution)/shard_map/ppermute | solution.py:29
  29.2 1.0 copy-start.3
  30.2 1.0 copy-start.4
  31.3 1.0 copy-start.5
  41.8 7.6 %collective-permute-start.11 = (bf16[64,2176]{1,0:T(8,128)(2,1)S(1)}, bf16[64,2176]{1,0:T(8,128)(2,1)S(1)}, u32[]{:S(2)}, u32[]{:S(2)}) collective-permute-start(bf16[64,2176]{1,0:T(8,128)(2,1)S(1)} %collective-permute-done.4.refs_0_), channel_id=1, source_target_pairs={{0,4},{1,5},{2,6},{3,7},{4,0},{5,1},{6,2},{7,3},{8,12},{9,13},{10,... | collective-permute-start | bytes 835592 | tf_op jit(solution)/shard_map/ppermute | solution.py:29
  42.3 7.5 %collective-permute-start.13 = (bf16[64,2176]{1,0:T(8,128)(2,1)S(1)}, bf16[64,2176]{1,0:T(8,128)(2,1)S(1)}, u32[]{:S(2)}, u32[]{:S(2)}) collective-permute-start(bf16[64,2176]{1,0:T(8,128)(2,1)S(1)} %collective-permute-done.4.refs_0_), channel_id=1, source_target_pairs={{0,8},{1,9},{2,10},{3,11},{4,12},{5,13},{6,14},{7,15},{8,0},{9,1},... | collective-permute-start | bytes 835592 | tf_op jit(solution)/shard_map/ppermute | solution.py:29
  49.8 6.7 %collective-permute-start.14 = (bf16[64,2176]{1,0:T(8,128)(2,1)S(1)}, bf16[64,2176]{1,0:T(8,128)(2,1)S(1)}, u32[]{:S(2)}, u32[]{:S(2)}) collective-permute-start(bf16[64,2176]{1,0:T(8,128)(2,1)S(1)} %collective-permute-done.13.refs_0_), channel_id=1, source_target_pairs={{0,4},{1,5},{2,6},{3,7},{4,0},{5,1},{6,2},{7,3},{8,12},{9,13},{10,... | collective-permute-start | bytes 835592 | tf_op jit(solution)/shard_map/ppermute | solution.py:29
  51.1 9.4 %collective-permute-start.18 = (bf16[64,2176]{1,0:T(8,128)(2,1)S(1)}, bf16[64,2176]{1,0:T(8,128)(2,1)S(1)}, u32[]{:S(2)}, u32[]{:S(2)}) collective-permute-start(bf16[64,2176]{1,0:T(8,128)(2,1)S(1)} %collective-permute-done.11.refs_1_), channel_id=1, source_target_pairs={{0,2},{1,3},{2,0},{3,1},{4,6},{5,7},{6,4},{7,5},{8,10},{9,11},{10,... | collective-permute-start | bytes 835592 | tf_op jit(solution)/shard_map/ppermute | solution.py:29
  51.9 11.6 %collective-permute-start.17 = (bf16[64,2176]{1,0:T(8,128)(2,1)S(1)}, bf16[64,2176]{1,0:T(8,128)(2,1)S(1)}, u32[]{:S(2)}, u32[]{:S(2)}) collective-permute-start(bf16[64,2176]{1,0:T(8,128)(2,1)S(1)} %collective-permute-done.4.refs_0_), channel_id=1, source_target_pairs={{0,2},{1,3},{2,0},{3,1},{4,6},{5,7},{6,4},{7,5},{8,10},{9,11},{10,... | collective-permute-start | bytes 835592 | tf_op jit(solution)/shard_map/ppermute | solution.py:29
  53.2 41.2 %collective-permute-start.23 = (bf16[128,2176]{1,0:T(8,128)(2,1)S(1)}, bf16[128,2176]{1,0:T(8,128)(2,1)S(1)}, u32[]{:S(2)}, u32[]{:S(2)}) collective-permute-start(bf16[128,2176]{1,0:T(8,128)(2,1)S(1)} %get-tuple-element.65.refs_0_), channel_id=1, source_target_pairs={{0,8},{1,9},{2,10},{3,11},{4,12},{5,13},{6,14},{7,15},{8,0},{9,1},... | collective-permute-start | bytes 1671176 | tf_op jit(solution)/shard_map/ppermute | solution.py:29
  54.8 39.5 %collective-permute-start.24 = (bf16[128,2176]{1,0:T(8,128)(2,1)S(1)}, bf16[128,2176]{1,0:T(8,128)(2,1)S(1)}, u32[]{:S(2)}, u32[]{:S(2)}) collective-permute-start(bf16[128,2176]{1,0:T(8,128)(2,1)S(1)} %collective-permute-done.12.refs_0_), channel_id=1, source_target_pairs={{0,8},{1,9},{2,10},{3,11},{4,12},{5,13},{6,14},{7,15},{8,0},{9,1},... | collective-permute-start | bytes 1671176 | tf_op jit(solution)/shard_map/ppermute | solution.py:29
  67.0 31.4 %collective-permute-start.22 = (bf16[128,2048]{1,0:T(8,128)(2,1)S(1)}, bf16[128,2048]{1,0:T(8,128)(2,1)S(1)}, u32[]{:S(2)}, u32[]{:S(2)}) collective-permute-start(bf16[128,2048]{1,0:T(8,128)(2,1)S(1)} %get-tuple-element.62), channel_id=1, source_target_pairs={{0,2},{1,3},{2,0},{3,1},{4,6},{5,7},{6,4},{7,5},{8,10},{9,11},{10,... | collective-permute-start | bytes 1572872 | tf_op jit(solution)/shard_map/ppermute | solution.py:29
  67.8 19.0 %collective-permute-start.20 = (bf16[64,2176]{1,0:T(8,128)(2,1)S(1)}, bf16[64,2176]{1,0:T(8,128)(2,1)S(1)}, u32[]{:S(2)}, u32[]{:S(2)}) collective-permute-start(bf16[64,2176]{1,0:T(8,128)(2,1)S(1)} %collective-permute-done.14.refs_2_), channel_id=1, source_target_pairs={{0,2},{1,3},{2,0},{3,1},{4,6},{5,7},{6,4},{7,5},{8,10},{9,11},{10,... | collective-permute-start | bytes 835592 | tf_op jit(solution)/shard_map/ppermute | solution.py:29
  69.1 20.7 %collective-permute-start.19 = (bf16[64,2176]{1,0:T(8,128)(2,1)S(1)}, bf16[64,2176]{1,0:T(8,128)(2,1)S(1)}, u32[]{:S(2)}, u32[]{:S(2)}) collective-permute-start(bf16[64,2176]{1,0:T(8,128)(2,1)S(1)} %collective-permute-done.13.refs_0_), channel_id=1, source_target_pairs={{0,2},{1,3},{2,0},{3,1},{4,6},{5,7},{6,4},{7,5},{8,10},{9,11},{10,... | collective-permute-start | bytes 835592 | tf_op jit(solution)/shard_map/ppermute | solution.py:29
  86.8 13.3 %collective-permute-start.15 = (bf16[128,2048]{1,0:T(8,128)(2,1)S(1)}, bf16[128,2048]{1,0:T(8,128)(2,1)S(1)}, u32[]{:S(2)}, u32[]{:S(2)}) collective-permute-start(bf16[128,2048]{1,0:T(8,128)(2,1)S(1)} %shard_map.139), channel_id=1, source_target_pairs={{0,4},{1,5},{2,6},{3,7},{4,0},{5,1},{6,2},{7,3},{8,12},{9,13},{10,... | collective-permute-start | bytes 1572872 | tf_op jit(solution)/shard_map/ppermute | solution.py:29
  93.5 16.5 %collective-permute-start.21 = (bf16[128,2048]{1,0:T(8,128)(2,1)S(1)}, bf16[128,2048]{1,0:T(8,128)(2,1)S(1)}, u32[]{:S(2)}, u32[]{:S(2)}) collective-permute-start(bf16[128,2048]{1,0:T(8,128)(2,1)S(1)} %get-tuple-element.64), channel_id=1, source_target_pairs={{0,4},{1,5},{2,6},{3,7},{4,0},{5,1},{6,2},{7,3},{8,12},{9,13},{10,... | collective-permute-start | bytes 1572872 | tf_op jit(solution)/shard_map/ppermute | solution.py:29
  97.9 21.4 %collective-permute-start.29 = (bf16[128,2048]{1,0:T(8,128)(2,1)S(1)}, bf16[128,2048]{1,0:T(8,128)(2,1)S(1)}, u32[]{:S(2)}, u32[]{:S(2)}) collective-permute-start(bf16[128,2048]{1,0:T(8,128)(2,1)S(1)} %get-tuple-element.67), channel_id=1, source_target_pairs={{0,2},{1,3},{2,0},{3,1},{4,6},{5,7},{6,4},{7,5},{8,10},{9,11},{10,... | collective-permute-start | bytes 1572872 | tf_op jit(solution)/shard_map/ppermute | solution.py:29
  98.5 14.3 %collective-permute-start.25 = (bf16[64,2048]{1,0:T(8,128)(2,1)S(1)}, bf16[64,2048]{1,0:T(8,128)(2,1)S(1)}, u32[]{:S(2)}, u32[]{:S(2)}) collective-permute-start(bf16[64,2048]{1,0:T(8,128)(2,1)S(1)} %add_convert_fusion.6), channel_id=1, source_target_pairs={{0,4},{1,5},{2,6},{3,7},{4,0},{5,1},{6,2},{7,3},{8,12},{9,13},{10,... | collective-permute-start | bytes 786440 | tf_op jit(solution)/shard_map/ppermute | solution.py:29
  100.2 27.0 %collective-permute-start.16 = (bf16[64,2048]{1,0:T(8,128)(2,1)S(1)}, bf16[64,2048]{1,0:T(8,128)(2,1)S(1)}, u32[]{:S(2)}, u32[]{:S(2)}) collective-permute-start(bf16[64,2048]{1,0:T(8,128)(2,1)S(1)} %get-tuple-element.75), channel_id=1, source_target_pairs={{0,2},{1,3},{2,0},{3,1},{4,6},{5,7},{6,4},{7,5},{8,10},{9,11},{10,... | collective-permute-start | bytes 786440 | tf_op jit(solution)/shard_map/ppermute | solution.py:29
  112.9 19.3 %collective-permute-start.26 = (bf16[64,2048]{1,0:T(8,128)(2,1)S(1)}, bf16[64,2048]{1,0:T(8,128)(2,1)S(1)}, u32[]{:S(2)}, u32[]{:S(2)}) collective-permute-start(bf16[64,2048]{1,0:T(8,128)(2,1)S(1)} %add_convert_fusion.5), channel_id=1, source_target_pairs={{0,16},{1,17},{2,18},{3,19},{4,20},{5,21},{6,22},{7,23},{8,24},{9,... | collective-permute-start | bytes 786440 | tf_op jit(solution)/shard_map/ppermute | solution.py:29
  118.5 6.4 %collective-permute-start.27 = (bf16[64,2048]{1,0:T(8,128)(2,1)S(1)}, bf16[64,2048]{1,0:T(8,128)(2,1)S(1)}, u32[]{:S(2)}, u32[]{:S(2)}) collective-permute-start(bf16[64,2048]{1,0:T(8,128)(2,1)S(1)} %add_convert_fusion.4), channel_id=1, source_target_pairs={{0,2},{1,3},{2,0},{3,1},{4,6},{5,7},{6,4},{7,5},{8,10},{9,11},{10,... | collective-permute-start | bytes 786440 | tf_op jit(solution)/shard_map/ppermute | solution.py:29
  119.4 6.4 %collective-permute-start.30 = (bf16[64,2048]{1,0:T(8,128)(2,1)S(1)}, bf16[64,2048]{1,0:T(8,128)(2,1)S(1)}, u32[]{:S(2)}, u32[]{:S(2)}) collective-permute-start(bf16[64,2048]{1,0:T(8,128)(2,1)S(1)} %add_convert_fusion.2), channel_id=1, source_target_pairs={{0,4},{1,5},{2,6},{3,7},{4,0},{5,1},{6,2},{7,3},{8,12},{9,13},{10,... | collective-permute-start | bytes 786440 | tf_op jit(solution)/shard_map/ppermute | solution.py:29
  125.0 9.5 %collective-permute-start.28 = (bf16[64,2048]{1,0:T(8,128)(2,1)S(1)}, bf16[64,2048]{1,0:T(8,128)(2,1)S(1)}, u32[]{:S(2)}, u32[]{:S(2)}) collective-permute-start(bf16[64,2048]{1,0:T(8,128)(2,1)S(1)} %add_convert_fusion.3), channel_id=1, source_target_pairs={{0,24},{1,25},{2,26},{3,27},{4,28},{5,29},{6,30},{7,31},{8,16},{9,... | collective-permute-start | bytes 786440 | tf_op jit(solution)/shard_map/ppermute | solution.py:29
  125.9 13.4 %collective-permute-start.31 = (bf16[64,2048]{1,0:T(8,128)(2,1)S(1)}, bf16[64,2048]{1,0:T(8,128)(2,1)S(1)}, u32[]{:S(2)}, u32[]{:S(2)}) collective-permute-start(bf16[64,2048]{1,0:T(8,128)(2,1)S(1)} %add_convert_fusion.1), channel_id=1, source_target_pairs={{0,8},{1,9},{2,10},{3,11},{4,12},{5,13},{6,14},{7,15},{8,0},{9,1},... | collective-permute-start | bytes 786440 | tf_op jit(solution)/shard_map/ppermute | solution.py:29
